TPU v7x, 32 devices: a whole 2x2x4 slice. The times are simulated.
32 devices in a mesh: grp: 2 (over y), ep: 8 (over z, x), tp: 2 (over core).
Axes of the slice: x: 2, y: 2, z: 4, core: 2. Of those that a mesh axis runs over, the one named last changes fastest.
Arguments:
- fresh_inputs: bfloat16 [256, 2048], P(('grp', 'ep')), parts along dimension 0, may hold values from -6 to 6
- memory_arrays: float32 [256, 32, 64, 64], P(('grp', 'ep'), 'tp'), parts along dimension 0, may hold values from -4 to 4
- chosen_specialist: int32 [256, 2], P(('grp', 'ep')), parts along dimension 0, may hold values from 0 to 3, all different within a row; in each aligned block of 128 rows (0 to 127, 128 to 255, ...) at most 96 rows name the same one
- chosen_coefficient: bfloat16 [256, 2], P(('grp', 'ep')), parts along dimension 0, may hold values from 0.25 to 1
- first_rescale: float32 [2048], replicated, may hold values from 0.1 to 1.9
- second_rescale: float32 [2048], replicated, may hold values from 0.1 to 1.9
- receiver_projector: bfloat16 [2048, 2048], P('tp', 'ep'), may hold values from -0.125 to 0.125
- address_projector: bfloat16 [2048, 2048], P('tp', 'ep'), may hold values from -0.125 to 0.125
- content_projector: bfloat16 [2048, 2048], P('tp', 'ep'), may hold values from -0.125 to 0.125
- final_projector: bfloat16 [2048, 2048], P('tp', 'ep'), may hold values from -0.125 to 0.125
- forget_narrowing: bfloat16 [2048, 64], replicated, may hold values from -0.125 to 0.125
- forget_widening: bfloat16 [64, 2048], P(None, 'tp'), may hold values from -0.75 to 0.75
- forget_bias: float32 [2048], P('tp'), may hold values from -3 to 1
- learning_narrowing: bfloat16 [2048, 64], replicated, may hold values from -0.125 to 0.125
- learning_widening: bfloat16 [64, 2048], P(None, 'tp'), may hold values from -0.75 to 0.75
- learning_bias: float32 [2048], P('tp'), may hold values from -1.5 to 1.5
- lane_scaling: float32 [2048], P('tp'), may hold values from 0.1 to 1.9
- instant_reward: float32 [32, 64], P('tp'), may hold values from -0.5 to 0.5
- specialist_switch: bfloat16 [2048, 28672], P(None, ('ep', 'tp')), may hold values from -0.125 to 0.125
- specialist_expand: bfloat16 [2048, 28672], P(None, ('ep', 'tp')), may hold values from -0.125 to 0.125
- specialist_contract: bfloat16 [28672, 2048], P(('ep', 'tp')), may hold values from -0.0625 to 0.0625
- common_activator: bfloat16 [2048, 5632], P(None, ('ep', 'tp')), may hold values from -0.125 to 0.125
- common_expand: bfloat16 [2048, 5632], P(None, ('ep', 'tp')), may hold values from -0.125 to 0.125
- common_contract: bfloat16 [5632, 2048], P(('ep', 'tp')), may hold values from -0.078125 to 0.078125
- common_switch: bfloat16 [2048], replicated, may hold values from -0.125 to 0.125
Outputs:
- new_tokens: bfloat16 [256, 2048], P(('grp', 'ep', 'tp')), parts along dimension 0
- memory_after: float32 [256, 32, 64, 64], P(('grp', 'ep'), 'tp'), parts along dimension 0
There are 2 independent parts, one for each index of `grp`. A program takes and returns all parts, laid end to end along the dimension named above; an argument that names none is the same for every part. Nothing has to cross between parts.
Inputs may be any that keep to these rules, and one draw needn't show every extreme that they name: `chosen_specialist`: each row names 2 different experts. Over the whole batch no expert is named by more than 96 rows, and in every draw some expert is named by exactly 96 rows.
All inputs are finite; a program needn't handle non-finite values.
Results may differ from a plain program's by a relative error of at most 0.014.
Values may be sent and summed in bfloat16 or wider, within the bound.
A program may use at most 128 MiB of HBM per device.

v0:
```python
import functools
import math

import jax
import jax.numpy as jnp
from jax import lax
from jax.experimental import pallas as pl
from jax.experimental.pallas import tpu as pltpu
from jax.sharding import PartitionSpec as P

LANE_WIDTH = 64
FF_E = 7168


RMS_EPS = 1e-06
GROUP_EPS = 0.00064
HIGHEST = lax.Precision.HIGHEST
MESH = pl.DeviceIdType.MESH
VMEM_ROOM = 40 * 2**20


def rms_norm(values, norm_gain):
    mean_sq = jnp.mean(values * values, axis=-1, keepdims=True)
    return values * lax.rsqrt(mean_sq + RMS_EPS) * norm_gain


def widen(rounded):
    return lax.optimization_barrier(rounded).astype(jnp.float32)


def evolve_memory(
    memory_arrays,
    receiver_lanes,
    address_lanes,
    content_lanes,
    forget_lanes,
    learning_lanes,
    lane_rescale,
    instant_reward,
):
    unit_key = address_lanes * lax.rsqrt(
        jnp.sum(address_lanes * address_lanes, axis=-1, keepdims=True) + 1.0
    )
    stepped_address = address_lanes * learning_lanes
    removal = jnp.einsum("bhvk,bhk->bhv", memory_arrays, unit_key, precision=HIGHEST)
    memory_after = (
        memory_arrays * forget_lanes[:, :, None, :]
        - removal[..., None] * (unit_key * learning_lanes)[:, :, None, :]
        + content_lanes[..., None] * stepped_address[:, :, None, :]
    )
    memory_retrieval = jnp.einsum("bhvk,bhk->bhv", memory_after, receiver_lanes, precision=HIGHEST)
    centred = memory_retrieval - jnp.mean(memory_retrieval, axis=-1, keepdims=True)
    unit_address = centred * lax.rsqrt(
        jnp.mean(centred * centred, axis=-1, keepdims=True) + GROUP_EPS
    )
    instant_extra = (
        jnp.sum(receiver_lanes * stepped_address * instant_reward, axis=-1, keepdims=True)
        * content_lanes
    )
    return (memory_after, unit_address * lane_rescale + instant_extra)


def swiglu(rows_in, gate_w, up_w):
    gate_val = jnp.dot(rows_in, gate_w, preferred_element_type=jnp.float32)
    up_val = jnp.dot(rows_in, up_w, preferred_element_type=jnp.float32)
    return (jax.nn.silu(gate_val) * up_val).astype(jnp.bfloat16)


def body(
    fresh_inputs,
    memory_arrays,
    chosen_specialist,
    chosen_coefficient,
    first_rescale,
    second_rescale,
    receiver_projector,
    address_projector,
    content_projector,
    final_projector,
    forget_narrowing,
    forget_widening,
    forget_bias,
    learning_narrowing,
    learning_widening,
    learning_bias,
    lane_scaling,
    instant_reward,
    specialist_switch,
    specialist_expand,
    specialist_contract,
    common_activator,
    common_expand,
    common_contract,
    common_switch,
):
    own_rows = fresh_inputs.shape[0]
    model_width = fresh_inputs.shape[1]
    tp_count = lax.axis_size("tp")
    tp_rank = lax.axis_index("tp")
    half_width = model_width // tp_count
    head_count = half_width // LANE_WIDTH
    residual = fresh_inputs.astype(jnp.float32)
    normed = rms_norm(residual, first_rescale).astype(jnp.bfloat16)
    normed_half = lax.dynamic_slice_in_dim(normed, tp_rank * half_width, half_width, 1)
    local_weights = jnp.stack((receiver_projector, address_projector, content_projector), axis=1)
    projected_rows = jnp.einsum(
        "rd,dkc->rkc",
        lax.all_gather(normed_half, "ep", axis=0, tiled=True),
        local_weights,
        preferred_element_type=jnp.float32,
    ).astype(jnp.bfloat16)
    partial_value = lax.all_to_all(projected_rows, "ep", split_axis=0, concat_axis=2, tiled=True)
    projected = lax.psum(widen(partial_value).astype(jnp.bfloat16), "tp")
    mine = lax.dynamic_slice_in_dim(projected, tp_rank * half_width, half_width, 2)

    def divide_lanes(channels):
        return channels.astype(jnp.float32).reshape(own_rows, head_count, LANE_WIDTH)

    decay_mid = jnp.tanh(
        jnp.dot(normed, forget_narrowing, preferred_element_type=jnp.float32)
    ).astype(jnp.bfloat16)
    decay_pre = forget_bias + jnp.dot(
        decay_mid, forget_widening, preferred_element_type=jnp.float32
    )
    decay_vals = jnp.exp(-jnp.exp(-jax.nn.softplus(-decay_pre) - 0.5))
    rate_mid = jnp.dot(normed, learning_narrowing, preferred_element_type=jnp.float32).astype(
        jnp.bfloat16
    )
    rate_vals = jax.nn.sigmoid(
        learning_bias + jnp.dot(rate_mid, learning_widening, preferred_element_type=jnp.float32)
    )
    memory_after, memory_retrieval = evolve_memory(
        memory_arrays,
        divide_lanes(mine[:, 0]),
        divide_lanes(mine[:, 1]),
        divide_lanes(mine[:, 2]),
        divide_lanes(decay_vals),
        divide_lanes(rate_vals),
        lane_scaling.reshape(head_count, LANE_WIDTH),
        instant_reward,
    )
    attended = memory_retrieval.reshape(own_rows, half_width).astype(jnp.bfloat16)
    done_rows = jnp.dot(
        lax.all_gather(attended, "ep", axis=0, tiled=True),
        final_projector,
        preferred_element_type=jnp.float32,
    ).astype(jnp.bfloat16)
    out_part = lax.all_to_all(done_rows, "ep", split_axis=0, concat_axis=1, tiled=True)
    mixed_out = lax.psum(widen(out_part).astype(jnp.bfloat16), "tp")
    residual = residual + mixed_out.astype(jnp.float32)
    ffn_in = rms_norm(residual, second_rescale).astype(jnp.bfloat16)
    all_in, all_weight, all_ids = (
        lax.all_gather(ffn_in, "ep", axis=0, tiled=True),
        lax.all_gather(chosen_coefficient, "ep", axis=0, tiled=True),
        lax.all_gather(chosen_specialist, "ep", axis=0, tiled=True),
    )
    column_count = specialist_switch.shape[1]
    flat_rank = lax.axis_index("ep") * tp_count + tp_rank
    expert = flat_rank * column_count // FF_E
    expert_share = jnp.sum(
        jnp.where(all_ids == expert, all_weight.astype(jnp.float32), 0.0), axis=1
    )
    hidden = swiglu(all_in, specialist_switch, specialist_expand)
    shared_hidden = swiglu(all_in, common_activator, common_expand)
    branch_scale = jax.nn.sigmoid(
        jnp.dot(all_in, common_switch, preferred_element_type=jnp.float32)
    )
    rows_mine = own_rows // tp_count
    expert_term = expert_share[:, None] * jnp.dot(
        hidden, specialist_contract, preferred_element_type=jnp.float32
    )
    routed = lax.psum_scatter(
        expert_term
        + branch_scale[:, None]
        * jnp.dot(shared_hidden, common_contract, preferred_element_type=jnp.float32),
        ("ep", "tp"),
        scatter_dimension=0,
        tiled=True,
    )
    own_residual = lax.dynamic_slice_in_dim(residual, tp_rank * rows_mine, rows_mine, 0)
    return ((own_residual + routed).astype(jnp.bfloat16), memory_after)


def _others(ep, tp, fn):
    me, core = lax.axis_index("ep"), lax.axis_index("tp")
    for far in range(ep):
        for side in range(tp):
            if far or side:
                fn(lax.rem(me + far, ep), lax.rem(core + side, tp))


def _greet(ep, tp):
    barrier = pltpu.get_barrier_semaphore()
    _others(
        ep,
        tp,
        lambda e, t: pl.semaphore_signal(
            barrier, inc=1, device_id={"ep": e, "tp": t}, device_id_type=MESH
        ),
    )


def _met(ep, tp):
    pl.semaphore_wait(pltpu.get_barrier_semaphore(), ep * tp - 1)


def _remote(src, dst, send, recv, e, t):
    return pltpu.make_async_remote_copy(
        src_ref=src,
        dst_ref=dst,
        send_sem=send,
        recv_sem=recv,
        device_id={"ep": e, "tp": t},
        device_id_type=MESH,
    )


def across_dot(left, right):
    return lax.dot_general(
        left, right, (((1,), (1,)), ((), ())), preferred_element_type=jnp.float32
    )


def by_head(ref, channels, first):
    for h in range(channels.shape[1] // LANE_WIDTH):
        ref[:, first + h, :] = channels[:, h * LANE_WIDTH : (h + 1) * LANE_WIDTH]


def round_dot(left, right, dims):
    return lax.dot_general(
        left.astype(jnp.bfloat16),
        right.astype(jnp.bfloat16),
        (dims, ((), ())),
        preferred_element_type=jnp.float32,
    )


def state_kernel(
    memory, query, key, value, decay, rate, lane_gain, reward, after, read, flip, probes, moves
):
    count, heads = query.shape[0], query.shape[1]
    lane = lax.broadcasted_iota(jnp.int32, (LANE_WIDTH, 128), 1)
    turn = lax.rem(lane, heads)
    chunk = math.gcd(heads, 4)

    def sequence(b):
        q, k, v, d, r = query[b], key[b], value[b], decay[b], rate[b]
        unit = k * lax.rsqrt(jnp.sum(k * k, axis=-1, keepdims=True) + 1.0)
        scaled, pulled, seen = k * r, unit * r, d * q
        flip[b, 2 * heads : 3 * heads] = v
        probes[b, 0:heads] = unit
        probes[b, heads : 2 * heads] = seen
        moves[b, 0:heads] = -pulled
        moves[b, 2 * heads : 3 * heads] = scaled
        value_cols = flip[b].T
        found = jnp.zeros((LANE_WIDTH, 128), jnp.float32)
        for first in range(0, heads, chunk):
            m = memory[b, first : first + chunk]
            sums = round_dot(m.reshape(chunk * LANE_WIDTH, LANE_WIDTH), probes[b], ((1,), (1,)))
            factors = []
            for i in range(chunk):
                both = sums[i * LANE_WIDTH : (i + 1) * LANE_WIDTH]
                both = jnp.where(lane < 2 * heads, both, value_cols)
                factors.append(jnp.where(turn == first + i, both, 0.0))
                found = found + factors[-1]
            change = round_dot(jnp.concatenate(factors, axis=0), moves[b], ((1,), (0,)))
            for i in range(chunk):
                h = first + i
                after[b, h] = m[i] * d[h : h + 1] + change[i * LANE_WIDTH : (i + 1) * LANE_WIDTH]
        rows = found.T
        out = (
            rows[heads : 2 * heads]
            - rows[0:heads] * jnp.sum(pulled * q, axis=-1, keepdims=True)
            + v * jnp.sum(scaled * q, axis=-1, keepdims=True)
        )
        centred = out - jnp.mean(out, axis=-1, keepdims=True)
        level = lax.rsqrt(jnp.mean(centred * centred, axis=-1, keepdims=True) + GROUP_EPS)
        extra = jnp.sum(q * scaled * reward[...], axis=-1, keepdims=True) * v
        read[b] = centred * level * lane_gain[...] + extra

    for ref in (flip, probes, moves):
        ref[...] = jnp.zeros_like(ref)
    for b in range(count):
        sequence(b)


def project_kernel(
    ep, tp, x, gain, wq, wk, wv, fnar, fwid, fbias, lnar, lwid, lbias, scaling,
    query, key, value, decay, rate, lane_gain,
    halves, rows_all, w, part, got, wsem, ssem, rsem, psem, gsem, lsem,
):
    me, core = lax.axis_index("ep"), lax.axis_index("tp")
    group = ep // tp
    _greet(ep, tp)
    loads = [pltpu.make_async_copy(ref, w.at[i], wsem.at[i]) for i, ref in enumerate((wq, wk, wv))]
    for load in loads:
        load.start()
    own, width = x.shape
    half = width // tp
    values = x[...].astype(jnp.float32)
    normed = (rms_norm(values, gain[...])).astype(jnp.bfloat16)
    for i in range(tp):
        halves[i] = normed[:, i * half : (i + 1) * half]
    _met(ep, tp)
    sends = []
    for far in range(1, ep):
        e = lax.rem(me + far, ep)
        sends.append(
            _remote(halves.at[core], rows_all.at[me], ssem.at[far], rsem.at[me], e, core)
        )
        sends[-1].start()
    rows_all[me] = halves[core]
    decay_mid = jnp.tanh(across_dot(normed, fnar[...])).astype(jnp.bfloat16)
    decay_pre = fbias[...] + jnp.dot(decay_mid, fwid[...], preferred_element_type=jnp.float32)
    by_head(decay, jnp.exp(-(math.exp(-0.5) / (1.0 + jnp.exp(-decay_pre)))), 0)
    rate_mid = across_dot(normed, lnar[...]).astype(jnp.bfloat16)
    rate_pre = lbias[...] + jnp.dot(rate_mid, lwid[...], preferred_element_type=jnp.float32)
    by_head(rate, 1.0 / (1.0 + jnp.exp(-rate_pre)), 0)
    for h in range(lane_gain.shape[0]):
        lane_gain[h : h + 1] = scaling[:, h * LANE_WIDTH : (h + 1) * LANE_WIDTH]
    for load in loads:
        load.wait()
    for far in range(1, ep):
        e = lax.rem(me + far, ep)
        pltpu.make_async_copy(rows_all.at[e], rows_all.at[e], rsem.at[e]).wait()
    every = rows_all[...].reshape(ep * own, half)
    for i in range(3):
        done = jnp.dot(every, w[i], preferred_element_type=jnp.float32)
        part[:, i] = done.astype(jnp.bfloat16).reshape(ep, own, done.shape[1])
    goal = me // group
    slot = core * group + lax.rem(me, group)
    for far in range(1, ep):
        e = lax.rem(me + far, ep)
        _remote(part.at[e], got.at[slot], psem.at[far], gsem.at[slot], e, goal).start()
    here = goal == core
    local = pltpu.make_async_copy(part.at[me], got.at[slot], gsem.at[slot])
    across = _remote(part.at[me], got.at[slot], psem.at[0], gsem.at[slot], me, goal)

    @pl.when(here)
    def _():
        local.start()

    @pl.when(jnp.logical_not(here))
    def _():
        across.start()

    for i in range(ep):
        pltpu.make_async_copy(got.at[i], got.at[i], gsem.at[i]).wait()
    cols = w.shape[2]
    for j in range(group):
        for i in range(3):
            total = got[j, i].astype(jnp.float32)
            for s in range(1, tp):
                total = total + got[s * group + j, i].astype(jnp.float32)
            total = total.astype(jnp.bfloat16).astype(jnp.float32)
            by_head((query, key, value)[i], total, j * (cols // LANE_WIDTH))
    for send in sends:
        send.wait_send()
    for far in range(1, ep):
        _remote(part.at[me], got.at[slot], psem.at[far], gsem.at[slot], me, goal).wait_send()

    @pl.when(jnp.logical_not(here))
    def _():
        across.wait_send()


def ffn_kernel(
    ep, tp, expert_cols, read, x, ids, coef, gain, cs, wo_h, wg_h, wu_h, wd_h, cg_h, cu_h, cd_h,
    out,
    att, att_all, xcol, share, wo, wg, wu, wd, cg, cu, cd, pbuf, psib, res, ffn, hid, chid,
    sibout, sibin, mine, got,
    wsem, s_att, r_att, s_x, r_x, s_sh, r_sh, s_p, r_p, s_res, r_res, f_res, b_res,
    s_sib, r_sib, s_out, r_out,
):
    me, core = lax.axis_index("ep"), lax.axis_index("tp")
    mate = lax.rem(core + 1, tp)
    group = ep // tp
    own, width = x.shape
    cols = wo.shape[1]
    _greet(ep, tp)
    loads = [
        pltpu.make_async_copy(a, b, wsem.at[i])
        for i, (a, b) in enumerate(
            ((wo_h, wo), (wg_h, wg), (wu_h, wu), (cg_h, cg), (cu_h, cu), (wd_h, wd), (cd_h, cd))
        )
    ]
    for load in loads:
        load.start()
    lane = lax.broadcasted_iota(jnp.int32, (own, 128), 1)
    routes = jnp.zeros((own, 128), jnp.float32)
    ids_cols, coef_cols = ids[...].T, coef[...].astype(jnp.float32).T
    for k in range(ids.shape[0]):
        routes = routes + jnp.where(
            ids_cols[:, k : k + 1] == lane, coef_cols[:, k : k + 1], 0.0
        )
    share[me] = routes.astype(jnp.bfloat16)
    pack = 128 // LANE_WIDTH
    for h in range(0, read.shape[1], pack):
        joined = jnp.concatenate([read[:, h + i, :] for i in range(pack)], axis=-1)
        att[:, h * LANE_WIDTH : h * LANE_WIDTH + 128] = joined.astype(jnp.bfloat16)
    _met(ep, tp)
    sends = []

    def push(*args):
        sends.append(_remote(*args))
        sends[-1].start()

    for far in range(1, ep):
        e = lax.rem(me + far, ep)
        push(att, att_all.at[me], s_att.at[far], r_att.at[me], e, core)
    side = me // group
    blocks = []
    for far in range(1, ep):
        e = lax.rem(me + far, ep)
        block = x.at[:, pl.ds(pl.multiple_of(e * cols, cols), cols)]
        blocks.append(_remote(block, xcol.at[me], s_x.at[far], r_x.at[me], e, core))

    @pl.when(side == core)
    def _():
        for copy in blocks:
            copy.start()

    for far in range(1, ep):
        e = lax.rem(me + far, ep)
        push(share.at[me], share.at[me], s_sh.at[far], r_sh.at[me], e, core)
    att_all[me] = att[...]
    xcol[me] = x[:, pl.ds(pl.multiple_of(me * cols, cols), cols)]
    loads[0].wait()

    def arrive(ref, sem):
        pltpu.make_async_copy(ref, ref, sem).wait()

    for far in range(1, ep):
        e = lax.rem(me + far, ep)
        arrive(att_all.at[e], r_att.at[e])
    half = att.shape[1]
    done = jnp.dot(
        att_all[...].reshape(ep * own, half), wo[...], preferred_element_type=jnp.float32
    ).astype(jnp.bfloat16)
    pbuf[...] = done.reshape(tp, group * own, cols)
    push(pbuf.at[mate], psib, s_p, r_p, me, mate)
    for j in range(group):
        e = core * group + j

        @pl.when(e != me)
        def _():
            arrive(xcol.at[e], r_x.at[e])

    arrive(psib, r_p)
    mixed = (pbuf[core].astype(jnp.float32) + psib[...].astype(jnp.float32)).astype(jnp.bfloat16)
    held = xcol[pl.ds(core * group, group)].reshape(group * own, cols).astype(jnp.float32)
    res[me, core] = (held + mixed.astype(jnp.float32)).astype(jnp.bfloat16)
    for far in range(1, ep):
        e = lax.rem(me + far, ep)
        push(res.at[me, core], res.at[me, core], s_res.at[far], r_res.at[me], e, core)
    push(res.at[me, core], res.at[me, core], f_res.at[me], b_res.at[me], me, mate)
    for far in range(1, ep):
        e = lax.rem(me + far, ep)
        arrive(res.at[e, core], r_res.at[e])
        push(res.at[e, core], res.at[e, core], f_res.at[e], b_res.at[e], me, mate)
    for far in range(ep):
        e = lax.rem(me + far, ep)
        arrive(res.at[e, mate], b_res.at[e])
    rows = ep * own
    square = jnp.zeros((rows, 1), jnp.float32)
    for s in range(ep):
        block = res[s].reshape(rows, cols).astype(jnp.float32)
        square = square + jnp.sum(block * block, axis=-1, keepdims=True)
    inv = lax.rsqrt(square / width + RMS_EPS)
    gate_sum = jnp.zeros((rows, 1), jnp.float32)
    for s in range(ep):
        at = slice(s * cols, (s + 1) * cols)
        block = res[s].reshape(rows, cols).astype(jnp.float32)
        block = (block * inv * gain[:, at]).astype(jnp.bfloat16)
        ffn[:, at] = block
        gate_sum = gate_sum + jnp.sum(
            block.astype(jnp.float32) * cs[:, at].astype(jnp.float32), axis=-1, keepdims=True
        )
    branch_scale = 1.0 / (1.0 + jnp.exp(-gate_sum))
    for far in range(1, ep):
        e = lax.rem(me + far, ep)
        arrive(share.at[e], r_sh.at[e])
    expert = (me * tp + core) * wg.shape[1] // expert_cols
    table = share[...].astype(jnp.float32).reshape(rows, 128)
    picked = lax.broadcasted_iota(jnp.int32, (rows, 128), 1) == expert
    weight = jnp.sum(jnp.where(picked, table, 0.0), axis=-1, keepdims=True)
    for i in (1, 2):
        loads[i].wait()

    def widen_up(c, _):
        at = pl.ds(pl.multiple_of(c * 256, 256), 256)
        g = jnp.dot(ffn[...], wg[:, at], preferred_element_type=jnp.float32)
        u = jnp.dot(ffn[...], wu[:, at], preferred_element_type=jnp.float32)
        hid[:, at] = (g / (1.0 + jnp.exp(-g)) * u).astype(jnp.bfloat16)
        return _

    lax.fori_loop(0, wg.shape[1] // 256, widen_up, 0)
    for i in (3, 4):
        loads[i].wait()
    g, u = across_dot(ffn[...], cg[...]), across_dot(ffn[...], cu[...])
    chid[...] = (g / (1.0 + jnp.exp(-g)) * u).astype(jnp.bfloat16)
    for i in (5, 6):
        loads[i].wait()
    pieces = mine.shape[0]
    piece = width // pieces
    last = own // tp
    for n in range(pieces):
        at = slice(n * piece, (n + 1) * piece)
        y = weight * jnp.dot(hid[...], wd[:, at], preferred_element_type=jnp.float32)
        y = y + branch_scale * jnp.dot(chid[...], cd[:, at], preferred_element_type=jnp.float32)
        y = y.reshape(ep, tp, last, piece)
        for k in range(tp):
            sibout[n, k] = y[:, k].astype(jnp.bfloat16)
        push(sibout.at[n, mate], sibin.at[n], s_sib.at[n], r_sib.at[n], me, mate)
    for n in range(pieces):
        arrive(sibin.at[n], r_sib.at[n])
        mine[n] = (
            sibout[n, core].astype(jnp.float32) + sibin[n].astype(jnp.float32)
        ).astype(jnp.bfloat16)
        for far in range(1, ep):
            e = lax.rem(me + far, ep)
            push(mine.at[n, e], got.at[n, me], s_out.at[n, far], r_out.at[n, me], e, core)
    start = pl.multiple_of(lax.rem(me, group) * own, own)
    per = piece // cols
    for n in range(pieces):
        total = mine[n, me].astype(jnp.float32)
        for far in range(1, ep):
            e = lax.rem(me + far, ep)
            arrive(got.at[n, e], r_out.at[n, e])
            total = total + got[n, e].astype(jnp.float32)
        for s in range(per):
            base = res[n * per + s, me // group, pl.ds(start, own)].astype(jnp.float32)
            base = jnp.where(core == 0, base[:last], base[last:])
            a = n * piece + s * cols
            out[:, a : a + cols] = (base + total[:, s * cols : (s + 1) * cols]).astype(jnp.bfloat16)
    for send in sends:
        send.wait_send()

    @pl.when(side == core)
    def _():
        for copy in blocks:
            copy.wait_send()


def layer(*blocks):
    own = blocks[0].shape[0]
    cols, hidden = blocks[9].shape[1], blocks[18].shape[1]
    heads = blocks[17].shape[0]
    tiles = cols % 128 == 0 and hidden % 256 == 0 and own % 16 == 0
    tiles = tiles and heads % 8 == 0 and 128 % heads == 0 and heads <= 32
    heads_match = lax.axis_size("ep") % lax.axis_size("tp") == 0 and lax.axis_size("tp") == 2
    weights = sum(2 * w.size for w in blocks[18:24])
    rows = own * lax.axis_size("ep")
    held = weights + rows * (12 * blocks[0].shape[1] + 8 * hidden)
    small = held < VMEM_ROOM
    return (kernel_body if tiles and heads_match and small else body)(*blocks)


def kernel_body(
    fresh_inputs,
    memory_arrays,
    chosen_specialist,
    chosen_coefficient,
    first_rescale,
    second_rescale,
    receiver_projector,
    address_projector,
    content_projector,
    final_projector,
    forget_narrowing,
    forget_widening,
    forget_bias,
    learning_narrowing,
    learning_widening,
    learning_bias,
    lane_scaling,
    instant_reward,
    specialist_switch,
    specialist_expand,
    specialist_contract,
    common_activator,
    common_expand,
    common_contract,
    common_switch,
):
    ep, tp = lax.axis_size("ep"), lax.axis_size("tp")
    own, width = fresh_inputs.shape
    half, cols = width // tp, final_projector.shape[1]
    heads = half // LANE_WIDTH
    group = ep // tp
    vmem = pl.BlockSpec(memory_space=pltpu.VMEM)
    hbm = pl.BlockSpec(memory_space=pl.ANY)
    bf16, f32 = jnp.bfloat16, jnp.float32
    dma = pltpu.SemaphoreType.DMA

    def row(vector):
        return vector.reshape(1, -1)

    per_head = jax.ShapeDtypeStruct((own, heads, LANE_WIDTH), f32)
    *lanes, lane_gain = pl.pallas_call(
        functools.partial(project_kernel, ep, tp),
        out_shape=(per_head,) * 5 + (jax.ShapeDtypeStruct((heads, LANE_WIDTH), f32),),
        in_specs=[vmem] * 2 + [hbm] * 3 + [vmem] * 7,
        out_specs=(vmem,) * 6,
        scratch_shapes=[
            pltpu.VMEM((tp, own, half), bf16),
            pltpu.VMEM((ep, own, half), bf16),
            pltpu.VMEM((3, half, cols), bf16),
            pltpu.VMEM((ep, 3, own, cols), bf16),
            pltpu.VMEM((ep, 3, own, cols), bf16),
            dma((3,)),
            dma((ep,)),
            dma((ep,)),
            dma((ep,)),
            dma((ep,)),
            dma((1,)),
        ],
        compiler_params=pltpu.CompilerParams(collective_id=0, has_side_effects=True),
        name="project",
    )(
        fresh_inputs,
        row(first_rescale),
        receiver_projector,
        address_projector,
        content_projector,
        forget_narrowing.T,
        forget_widening,
        row(forget_bias),
        learning_narrowing.T,
        learning_widening,
        row(learning_bias),
        row(lane_scaling),
    )
    step = 2
    lane_spec = pl.BlockSpec((step, heads, LANE_WIDTH), lambda i: (i, 0, 0))
    gain_spec = pl.BlockSpec((heads, LANE_WIDTH), lambda i: (0, 0))
    memory_spec = pl.BlockSpec((step, heads, LANE_WIDTH, LANE_WIDTH), lambda i: (i, 0, 0, 0))
    memory_after, read = pl.pallas_call(
        state_kernel,
        grid=(own // step,),
        out_shape=(jax.ShapeDtypeStruct(memory_arrays.shape, f32), per_head),
        in_specs=[memory_spec] + [lane_spec] * 5 + [gain_spec] * 2,
        out_specs=(memory_spec, lane_spec),
        scratch_shapes=[pltpu.VMEM((step, 128, LANE_WIDTH), f32)] * 3,
        name="state",
    )(memory_arrays, *lanes, lane_gain, instant_reward)
    rows, hidden, dense = ep * own, specialist_switch.shape[1], common_activator.shape[1]
    pieces = 4
    piece, last = width // pieces, own // tp
    new_tokens = pl.pallas_call(
        functools.partial(ffn_kernel, ep, tp, FF_E),
        out_shape=jax.ShapeDtypeStruct((last, width), bf16),
        in_specs=[vmem] * 6 + [hbm] * 7,
        out_specs=vmem,
        scratch_shapes=[
            pltpu.VMEM((own, half), bf16),
            pltpu.VMEM((ep, own, half), bf16),
            pltpu.VMEM((ep, own, cols), bf16),
            pltpu.VMEM((ep, own, 128), bf16),
            pltpu.VMEM((half, cols), bf16),
            pltpu.VMEM((width, hidden), bf16),
            pltpu.VMEM((width, hidden), bf16),
            pltpu.VMEM((hidden, width), bf16),
            pltpu.VMEM((dense, width), bf16),
            pltpu.VMEM((dense, width), bf16),
            pltpu.VMEM((dense, width), bf16),
            pltpu.VMEM((tp, group * own, cols), bf16),
            pltpu.VMEM((group * own, cols), bf16),
            pltpu.VMEM((ep, tp, group * own, cols), bf16),
            pltpu.VMEM((rows, width), bf16),
            pltpu.VMEM((rows, hidden), bf16),
            pltpu.VMEM((rows, dense), bf16),
            pltpu.VMEM((pieces, tp, ep, last, piece), bf16),
            pltpu.VMEM((pieces, ep, last, piece), bf16),
            pltpu.VMEM((pieces, ep, last, piece), bf16),
            pltpu.VMEM((pieces, ep, last, piece), bf16),
            dma((7,)),
            dma((ep,)),
            dma((ep,)),
            dma((ep,)),
            dma((ep,)),
            dma((ep,)),
            dma((ep,)),
            dma,
            dma,
            dma((ep,)),
            dma((ep,)),
            dma((ep,)),
            dma((ep,)),
            dma((pieces,)),
            dma((pieces,)),
            dma((pieces, ep)),
            dma((pieces, ep)),
        ],
        compiler_params=pltpu.CompilerParams(
            collective_id=1, has_side_effects=True, vmem_limit_bytes=56 * 2**20
        ),
        name="experts",
    )(
        read,
        fresh_inputs,
        chosen_specialist.T,
        chosen_coefficient.T,
        row(second_rescale),
        row(common_switch),
        final_projector,
        specialist_switch,
        specialist_expand,
        specialist_contract,
        common_activator.T,
        common_expand.T,
        common_contract,
    )
    return (new_tokens, memory_after)


def solution(mesh):
    placed = (
        P(("grp", "ep"), None),
        P(("grp", "ep"), "tp", None, None),
        P(("grp", "ep"), None),
        P(("grp", "ep"), None),
        P(),
        P(),
        P("tp", "ep"),
        P("tp", "ep"),
        P("tp", "ep"),
        P("tp", "ep"),
        P(),
        P(None, "tp"),
        P("tp"),
        P(),
        P(None, "tp"),
        P("tp"),
        P("tp"),
        P("tp", None),
        P(None, ("ep", "tp")),
        P(None, ("ep", "tp")),
        P(("ep", "tp"), None),
        P(None, ("ep", "tp")),
        P(None, ("ep", "tp")),
        P(("ep", "tp"), None),
        P(),
    )
    return jax.shard_map(
        layer,
        mesh=mesh,
        in_specs=placed,
        out_specs=(P(("grp", "ep", "tp"), None), P(("grp", "ep"), "tp", None, None)),
        check_vma=False,
    )
```

profile of v0, /device:TPU:0, one launch (start us, length us, event | category | flops | bytes accessed | tf_op | source)
XLA Modules:
  0.0 76.1 jit_solution(1225130195691674703)
XLA Ops:
  0.6 0.0 copy-start
  0.6 20.6 %project.1 = (f32[16,16,64]{2,1,0:T(8,128)}, f32[16,16,64]{2,1,0:T(8,128)}, f32[16,16,64]{2,1,0:T(8,128)}, f32[16,16,64]{2,1,0:T(8,128)}, f32[16,16,64]{2,1,0:T(8,128)}, /*index=5*/f32[16,64]{1,0:T(8,128)}) custom-call(bf16[16,2048]{1,0:T(8,128)(2,1)} %x.3, f32[1,2048]{1,0:T(1,128)} %bitcast.15, bf16[1024,256]{1,0:T(8,128)(2,1)} %wq.1, ...), custom_call_target="tpu_custom_call" | custom-call | tf_op jit(solution)/shard_map/project/pallas_call | solution.py:600
  21.3 11.7 %state.1 = (f32[16,16,64,64]{3,2,1,0:T(8,128)}, f32[16,16,64]{2,1,0:T(8,128)}) custom-call(f32[16,16,64,64]{3,2,1,0:T(8,128)} %memory.1, f32[16,16,64]{2,1,0:T(8,128)} %get-tuple-element.10.query, f32[16,16,64]{2,1,0:T(8,128)} %get-tuple-element.11.key, f32[16,16,64]{2,1,0:T(8,128)} %get-tuple-element.12.value, f32[16,16,64]{2,1,0:T(8,128)} %get-tuple-element.13.decay, ...), custom_call_target="tpu_custom_call" | custom-call | tf_op jit(solution)/shard_map/state/pallas_call | solution.py:638
  33.0 0.0 copy-done
  33.0 0.6 reshape.27.cs
  33.6 41.1 %experts.1 = bf16[8,2048]{1,0:T(8,128)(2,1)} custom-call(f32[16,16,64]{2,1,0:T(8,128)} %get-tuple-element.16.read, bf16[16,2048]{1,0:T(8,128)(2,1)} %x.3, s32[2,16]{1,0:T(2,128)} %bitcast.20, bf16[2,16]{1,0:T(2,128)(2,1)} %bitcast.21, f32[1,2048]{1,0:T(1,128)} %bitcast.16, bf16[1,2048]{1,0:T(2,128)(2,1)} %reshape.27.cs, bf16[1024,256]{1,0:T(8,128)(2,1)} %wo_h.1, ...), custom_call_target="tpu_custom_call" | custom-call | tf_op jit(solution)/shard_map/experts/pallas_call | solution.py:650
  74.7 1.4 %copy.28 = bf16[8,2048]{1,0:T(8,128)(2,1)} copy(bf16[8,2048]{1,0:T(8,128)(2,1)} %experts.1) | data formatting | bytes 65536
Async XLA Ops:
  0.6 32.3 %copy-start = (bf16[2048]{0:T(1024)(128)(2,1)S(1)}, bf16[2048]{0:T(1024)(128)(2,1)}, u32[]{:S(2)}) copy-start(bf16[2048]{0:T(1024)(128)(2,1)} %param.49) | copy-start | bytes 12292
where the time goes:
time: 76.5 us; the launch traced here: 76.1 us
  Pallas kernels  73.4 us (96%)
  local copies, waits for them, and re-layouts  1.98 us (3%)
    pallas_call x1, Pallas kernels, kernel_body(): pl.pallas_call(functools.partial(ffn_kernel, ep, tp, FF_E), out_shape=jax...  41.1 us
    pallas_call x1, Pallas kernels, kernel_body(): pl.pallas_call(functools.partial(project_kernel, ep, tp), out_shape=(per_...  20.6 us
    pallas_call x1, Pallas kernels, kernel_body(): pl.pallas_call(state_kernel, grid=(own // step,), out_shape=(jax.ShapeDty...  11.7 us

commit v1 on v0

v1 whole, which is shorter than its diff:
```python
import functools
import math

import jax
import jax.numpy as jnp
from jax import lax
from jax.experimental import pallas as pl
from jax.experimental.pallas import tpu as pltpu
from jax.sharding import PartitionSpec as P

LANE_WIDTH = 64
FF_E = 7168


RMS_EPS = 1e-06
GROUP_EPS = 0.00064
HIGHEST = lax.Precision.HIGHEST
MESH = pl.DeviceIdType.MESH
VMEM_ROOM = 52 * 2**20


def rms_norm(values, norm_gain):
    mean_sq = jnp.mean(values * values, axis=-1, keepdims=True)
    return values * lax.rsqrt(mean_sq + RMS_EPS) * norm_gain


def widen(rounded):
    return lax.optimization_barrier(rounded).astype(jnp.float32)


def evolve_memory(
    memory_arrays,
    receiver_lanes,
    address_lanes,
    content_lanes,
    forget_lanes,
    learning_lanes,
    lane_rescale,
    instant_reward,
):
    unit_key = address_lanes * lax.rsqrt(
        jnp.sum(address_lanes * address_lanes, axis=-1, keepdims=True) + 1.0
    )
    stepped_address = address_lanes * learning_lanes
    removal = jnp.einsum("bhvk,bhk->bhv", memory_arrays, unit_key, precision=HIGHEST)
    memory_after = (
        memory_arrays * forget_lanes[:, :, None, :]
        - removal[..., None] * (unit_key * learning_lanes)[:, :, None, :]
        + content_lanes[..., None] * stepped_address[:, :, None, :]
    )
    memory_retrieval = jnp.einsum("bhvk,bhk->bhv", memory_after, receiver_lanes, precision=HIGHEST)
    centred = memory_retrieval - jnp.mean(memory_retrieval, axis=-1, keepdims=True)
    unit_address = centred * lax.rsqrt(
        jnp.mean(centred * centred, axis=-1, keepdims=True) + GROUP_EPS
    )
    instant_extra = (
        jnp.sum(receiver_lanes * stepped_address * instant_reward, axis=-1, keepdims=True)
        * content_lanes
    )
    return (memory_after, unit_address * lane_rescale + instant_extra)


def swiglu(rows_in, gate_w, up_w):
    gate_val = jnp.dot(rows_in, gate_w, preferred_element_type=jnp.float32)
    up_val = jnp.dot(rows_in, up_w, preferred_element_type=jnp.float32)
    return (jax.nn.silu(gate_val) * up_val).astype(jnp.bfloat16)


def body(
    fresh_inputs,
    memory_arrays,
    chosen_specialist,
    chosen_coefficient,
    first_rescale,
    second_rescale,
    receiver_projector,
    address_projector,
    content_projector,
    final_projector,
    forget_narrowing,
    forget_widening,
    forget_bias,
    learning_narrowing,
    learning_widening,
    learning_bias,
    lane_scaling,
    instant_reward,
    specialist_switch,
    specialist_expand,
    specialist_contract,
    common_activator,
    common_expand,
    common_contract,
    common_switch,
):
    own_rows = fresh_inputs.shape[0]
    model_width = fresh_inputs.shape[1]
    tp_count = lax.axis_size("tp")
    tp_rank = lax.axis_index("tp")
    half_width = model_width // tp_count
    head_count = half_width // LANE_WIDTH
    residual = fresh_inputs.astype(jnp.float32)
    normed = rms_norm(residual, first_rescale).astype(jnp.bfloat16)
    normed_half = lax.dynamic_slice_in_dim(normed, tp_rank * half_width, half_width, 1)
    local_weights = jnp.stack((receiver_projector, address_projector, content_projector), axis=1)
    projected_rows = jnp.einsum(
        "rd,dkc->rkc",
        lax.all_gather(normed_half, "ep", axis=0, tiled=True),
        local_weights,
        preferred_element_type=jnp.float32,
    ).astype(jnp.bfloat16)
    partial_value = lax.all_to_all(projected_rows, "ep", split_axis=0, concat_axis=2, tiled=True)
    projected = lax.psum(widen(partial_value).astype(jnp.bfloat16), "tp")
    mine = lax.dynamic_slice_in_dim(projected, tp_rank * half_width, half_width, 2)

    def divide_lanes(channels):
        return channels.astype(jnp.float32).reshape(own_rows, head_count, LANE_WIDTH)

    decay_mid = jnp.tanh(
        jnp.dot(normed, forget_narrowing, preferred_element_type=jnp.float32)
    ).astype(jnp.bfloat16)
    decay_pre = forget_bias + jnp.dot(
        decay_mid, forget_widening, preferred_element_type=jnp.float32
    )
    decay_vals = jnp.exp(-jnp.exp(-jax.nn.softplus(-decay_pre) - 0.5))
    rate_mid = jnp.dot(normed, learning_narrowing, preferred_element_type=jnp.float32).astype(
        jnp.bfloat16
    )
    rate_vals = jax.nn.sigmoid(
        learning_bias + jnp.dot(rate_mid, learning_widening, preferred_element_type=jnp.float32)
    )
    memory_after, memory_retrieval = evolve_memory(
        memory_arrays,
        divide_lanes(mine[:, 0]),
        divide_lanes(mine[:, 1]),
        divide_lanes(mine[:, 2]),
        divide_lanes(decay_vals),
        divide_lanes(rate_vals),
        lane_scaling.reshape(head_count, LANE_WIDTH),
        instant_reward,
    )
    attended = memory_retrieval.reshape(own_rows, half_width).astype(jnp.bfloat16)
    done_rows = jnp.dot(
        lax.all_gather(attended, "ep", axis=0, tiled=True),
        final_projector,
        preferred_element_type=jnp.float32,
    ).astype(jnp.bfloat16)
    out_part = lax.all_to_all(done_rows, "ep", split_axis=0, concat_axis=1, tiled=True)
    mixed_out = lax.psum(widen(out_part).astype(jnp.bfloat16), "tp")
    residual = residual + mixed_out.astype(jnp.float32)
    ffn_in = rms_norm(residual, second_rescale).astype(jnp.bfloat16)
    all_in, all_weight, all_ids = (
        lax.all_gather(ffn_in, "ep", axis=0, tiled=True),
        lax.all_gather(chosen_coefficient, "ep", axis=0, tiled=True),
        lax.all_gather(chosen_specialist, "ep", axis=0, tiled=True),
    )
    column_count = specialist_switch.shape[1]
    flat_rank = lax.axis_index("ep") * tp_count + tp_rank
    expert = flat_rank * column_count // FF_E
    expert_share = jnp.sum(
        jnp.where(all_ids == expert, all_weight.astype(jnp.float32), 0.0), axis=1
    )
    hidden = swiglu(all_in, specialist_switch, specialist_expand)
    shared_hidden = swiglu(all_in, common_activator, common_expand)
    branch_scale = jax.nn.sigmoid(
        jnp.dot(all_in, common_switch, preferred_element_type=jnp.float32)
    )
    rows_mine = own_rows // tp_count
    expert_term = expert_share[:, None] * jnp.dot(
        hidden, specialist_contract, preferred_element_type=jnp.float32
    )
    routed = lax.psum_scatter(
        expert_term
        + branch_scale[:, None]
        * jnp.dot(shared_hidden, common_contract, preferred_element_type=jnp.float32),
        ("ep", "tp"),
        scatter_dimension=0,
        tiled=True,
    )
    own_residual = lax.dynamic_slice_in_dim(residual, tp_rank * rows_mine, rows_mine, 0)
    return ((own_residual + routed).astype(jnp.bfloat16), memory_after)


def flipped(index, mask):
    for bit in range(mask.bit_length()):
        step = 1 << bit
        if mask & step:
            index = index + step * (1 - 2 * lax.rem(index // step, 2))
    return index


def _greet(ep, tp):
    me, core = lax.axis_index("ep"), lax.axis_index("tp")
    barrier = pltpu.get_barrier_semaphore()
    for mask in range(ep - 1, -1, -1):
        for side in range(tp):
            if mask or side:
                pl.semaphore_signal(
                    barrier,
                    inc=1,
                    device_id={"ep": flipped(me, mask), "tp": lax.rem(core + side, tp)},
                    device_id_type=MESH,
                )


def _met(ep, tp):
    pl.semaphore_wait(pltpu.get_barrier_semaphore(), ep * tp - 1)


def _remote(src, dst, send, recv, e, t):
    return pltpu.make_async_remote_copy(
        src_ref=src,
        dst_ref=dst,
        send_sem=send,
        recv_sem=recv,
        device_id={"ep": e, "tp": t},
        device_id_type=MESH,
    )


def across_dot(left, right):
    return lax.dot_general(
        left, right, (((1,), (1,)), ((), ())), preferred_element_type=jnp.float32
    )


def by_head(ref, channels, first):
    for h in range(channels.shape[1] // LANE_WIDTH):
        ref[:, first + h, :] = channels[:, h * LANE_WIDTH : (h + 1) * LANE_WIDTH]


def arrive(ref, sem):
    pltpu.make_async_copy(ref, ref, sem).wait()


def layer_kernel(
    ep, tp, expert_cols,
    x_h, memory, ids_h, coef_h, gain_h, gain2_h, cs_h, reward_h, scaling_h,
    wq_h, wk_h, wv_h, wo_h, fnar_h, fwid_h, fbias_h, lnar_h, lwid_h, lbias_h,
    wg_h, wu_h, wd_h, cg_h, cu_h, cd_h,
    out, mem,
    x, ids, coef, gain, gain2, cs, reward, scaling, fnar, fwid, fbias, lnar, lwid, lbias,
    w, wo, wg, wu, wd, cg, cu, cd, pk, pk16,
    halves, rows_all, part, gotp, query, key, value, decay, rate, dch, lane_gain,
    flip, probes, moves, factors, read,
    att, att_all, xcol, share, pbuf, psib, res, ffn, hid, chid, sibout, sibin, mine, got,
    lsem, msem, wsem,
    s_row, r_row, s_part, r_part, s_att, r_att, s_x, r_x, s_sh, r_sh, s_p, r_p,
    s_res, r_res, f_res, b_res, s_sib, r_sib, s_out, r_out,
):
    me, core = lax.axis_index("ep"), lax.axis_index("tp")
    mate = lax.rem(core + 1, tp)
    group = ep // tp
    side = me // group
    own, width = x.shape
    half = width // tp
    cols = wo.shape[1]
    rows = ep * own
    heads = lane_gain.shape[0]
    pack = pk.shape[2] // LANE_WIDTH
    packs = heads // pack
    block_rows = packs * LANE_WIDTH
    far = list(range(ep - 1, 0, -1))
    _greet(ep, tp)

    smalls = [
        pltpu.make_async_copy(a, b, lsem.at[i])
        for i, (a, b) in enumerate(
            (
                (x_h, x), (gain_h, gain), (fnar_h, fnar), (fwid_h, fwid), (fbias_h, fbias),
                (lnar_h, lnar), (lwid_h, lwid), (lbias_h, lbias), (scaling_h, scaling),
                (reward_h, reward), (ids_h, ids), (coef_h, coef), (gain2_h, gain2), (cs_h, cs),
            )
        )
    ]
    weights = [
        pltpu.make_async_copy(a, b, wsem.at[i])
        for i, (a, b) in enumerate(
            (
                (wq_h, w.at[0]), (wk_h, w.at[1]), (wv_h, w.at[2]), (wo_h, wo), (wg_h, wg),
                (wu_h, wu), (cg_h, cg), (cu_h, cu), (wd_h, wd), (cd_h, cd),
            )
        )
    ]
    batches = msem.shape[0]
    batch = own // batches
    states = [
        pltpu.make_async_copy(
            memory.at[pl.ds(i * batch, batch)], mem.at[pl.ds(i * batch, batch)], msem.at[i]
        )
        for i in range(batches)
    ]
    for copy in smalls + weights[:3] + states:
        copy.start()
    sends = []

    def push(*args):
        sends.append(_remote(*args))
        sends[-1].start()

    for copy in smalls[:2]:
        copy.wait()
    normed = rms_norm(x[...].astype(jnp.float32), gain[...]).astype(jnp.bfloat16)
    for i in range(tp):
        halves[i] = normed[:, i * half : (i + 1) * half]
    _met(ep, tp)
    for k in far:
        push(halves.at[core], rows_all.at[me], s_row.at[k], r_row.at[me], flipped(me, k), core)
    rows_all[me] = halves[core]

    for copy in smalls[2:]:
        copy.wait()
    decay_mid = jnp.tanh(across_dot(normed, fnar[...])).astype(jnp.bfloat16)
    decay_pre = fbias[...] + jnp.dot(decay_mid, fwid[...], preferred_element_type=jnp.float32)
    kept = jnp.exp(-(math.exp(-0.5) / (1.0 + jnp.exp(-decay_pre))))
    dch[...] = kept
    by_head(decay, kept, 0)
    rate_mid = across_dot(normed, lnar[...]).astype(jnp.bfloat16)
    rate_pre = lbias[...] + jnp.dot(rate_mid, lwid[...], preferred_element_type=jnp.float32)
    by_head(rate, 1.0 / (1.0 + jnp.exp(-rate_pre)), 0)
    for h in range(heads):
        lane_gain[h : h + 1] = scaling[:, h * LANE_WIDTH : (h + 1) * LANE_WIDTH]
    for ref in (flip, probes, moves):
        ref[...] = jnp.zeros_like(ref)
    lane = lax.broadcasted_iota(jnp.int32, (own, 128), 1)
    routes = jnp.zeros((own, 128), jnp.float32)
    ids_cols, coef_cols = ids[...].T, coef[...].astype(jnp.float32).T
    for i in range(ids.shape[0]):
        routes = routes + jnp.where(
            ids_cols[:, i : i + 1] == lane, coef_cols[:, i : i + 1], 0.0
        )
    share[me] = routes.astype(jnp.bfloat16)
    xcol[me] = x[:, pl.ds(pl.multiple_of(me * cols, cols), cols)]
    for copy in states:
        copy.wait()
    for copy in weights[3:]:
        copy.start()

    def join(b, _):
        for p in range(packs):
            joined = jnp.concatenate([mem[b, p * pack + i] for i in range(pack)], axis=-1)
            at = slice(p * LANE_WIDTH, (p + 1) * LANE_WIDTH)
            pk[b, at] = joined
            pk16[b, at] = joined.astype(jnp.bfloat16)
        return _

    lax.fori_loop(0, own, join, 0)

    for copy in weights[:3]:
        copy.wait()
    for k in far:
        e = flipped(me, k)
        arrive(rows_all.at[e], r_row.at[e])
    every = rows_all[...].reshape(rows, half)
    for i in range(3):
        done = jnp.dot(every, w[i], preferred_element_type=jnp.float32)
        part[:, i] = done.astype(jnp.bfloat16).reshape(ep, own, cols)
    slot = core * group + lax.rem(me, group)
    for k in far:
        e = flipped(me, k)
        push(part.at[e], gotp.at[slot], s_part.at[k], r_part.at[slot], e, side)
    here = side == core
    local = pltpu.make_async_copy(part.at[me], gotp.at[slot], r_part.at[slot])
    across = _remote(part.at[me], gotp.at[slot], s_part.at[0], r_part.at[slot], me, side)

    @pl.when(here)
    def _():
        local.start()

    @pl.when(jnp.logical_not(here))
    def _():
        across.start()

    blocks = []
    for k in far:
        e = flipped(me, k)
        block = x.at[:, pl.ds(pl.multiple_of(e * cols, cols), cols)]
        blocks.append(_remote(block, xcol.at[me], s_x.at[k], r_x.at[me], e, core))

    @pl.when(here)
    def _():
        for copy in blocks:
            copy.start()

    for k in far:
        push(share.at[me], share.at[me], s_sh.at[k], r_sh.at[me], flipped(me, k), core)

    for j in range(group):
        for s in range(tp):
            arrive(gotp.at[s * group + j], r_part.at[s * group + j])
        for i in range(3):
            total = gotp[j, i].astype(jnp.float32)
            for s in range(1, tp):
                total = total + gotp[s * group + j, i].astype(jnp.float32)
            total = total.astype(jnp.bfloat16).astype(jnp.float32)
            by_head((query, key, value)[i], total, j * (cols // LANE_WIDTH))

    wide = pack * LANE_WIDTH
    placed = lax.rem(
        lax.broadcasted_iota(jnp.int32, (heads, wide), 0), pack
    ) == lax.broadcasted_iota(jnp.int32, (heads, wide), 1) // LANE_WIDTH
    vlane = lax.broadcasted_iota(jnp.int32, (LANE_WIDTH, 128), 1)
    turn = lax.rem(vlane, heads) // pack

    def spread(channels):
        return jnp.where(placed, jnp.concatenate([channels] * pack, axis=-1), 0.0).astype(
            jnp.bfloat16
        )

    for b in range(own):
        q, k, v, r = query[b], key[b], value[b], rate[b]
        unit = k * lax.rsqrt(jnp.sum(k * k, axis=-1, keepdims=True) + 1.0)
        scaled, pulled, seen = k * r, unit * r, decay[b] * q
        flip[b, 2 * heads : 3 * heads] = v
        probes[b, 0:heads] = spread(unit)
        probes[b, heads : 2 * heads] = spread(seen)
        moves[b, 0:heads] = spread(-pulled)
        moves[b, 2 * heads : 3 * heads] = spread(scaled)
        value_cols = flip[b].T
        sums = across_dot(pk16[b], probes[b])
        found = jnp.zeros((LANE_WIDTH, 128), jnp.float32)
        for p in range(packs):
            at = slice(p * LANE_WIDTH, (p + 1) * LANE_WIDTH)
            both = jnp.where(vlane < 2 * heads, sums[at], value_cols)
            both = jnp.where(turn == p, both, 0.0)
            factors[b, at] = both.astype(jnp.bfloat16)
            found = found + both
        turned = found.T
        seen_rows = (
            turned[heads : 2 * heads]
            - turned[0:heads] * jnp.sum(pulled * q, axis=-1, keepdims=True)
            + v * jnp.sum(scaled * q, axis=-1, keepdims=True)
        )
        centred = seen_rows - jnp.mean(seen_rows, axis=-1, keepdims=True)
        level = lax.rsqrt(jnp.mean(centred * centred, axis=-1, keepdims=True) + GROUP_EPS)
        extra = jnp.sum(q * scaled * reward[...], axis=-1, keepdims=True) * v
        read[b] = centred * level * lane_gain[...] + extra
    for h in range(0, heads, 2):
        joined = jnp.concatenate([read[:, h + i, :] for i in range(2)], axis=-1)
        att[:, h * LANE_WIDTH : (h + 2) * LANE_WIDTH] = joined.astype(jnp.bfloat16)
    for k in far:
        push(att, att_all.at[me], s_att.at[k], r_att.at[me], flipped(me, k), core)
    att_all[me] = att[...]

    def renew(b, _):
        change = jnp.dot(factors[b], moves[b], preferred_element_type=jnp.float32)
        for p in range(packs):
            at = slice(p * LANE_WIDTH, (p + 1) * LANE_WIDTH)
            new = pk[b, at] * dch[pl.ds(b, 1), p * wide : (p + 1) * wide] + change[at]
            for i in range(pack):
                mem[b, p * pack + i] = new[:, i * LANE_WIDTH : (i + 1) * LANE_WIDTH]
        return _

    lax.fori_loop(0, own, renew, 0)

    weights[3].wait()
    for k in far:
        e = flipped(me, k)
        arrive(att_all.at[e], r_att.at[e])
    done = jnp.dot(
        att_all[...].reshape(rows, half), wo[...], preferred_element_type=jnp.float32
    ).astype(jnp.bfloat16)
    pbuf[...] = done.reshape(tp, group * own, cols)
    push(pbuf.at[mate], psib, s_p, r_p, me, mate)
    for j in range(group):
        e = core * group + j

        @pl.when(e != me)
        def _():
            arrive(xcol.at[e], r_x.at[e])

    arrive(psib, r_p)
    mixed = (pbuf[core].astype(jnp.float32) + psib[...].astype(jnp.float32)).astype(jnp.bfloat16)
    held = xcol[pl.ds(core * group, group)].reshape(group * own, cols).astype(jnp.float32)
    res[me, core] = (held + mixed.astype(jnp.float32)).astype(jnp.bfloat16)
    for k in far:
        push(res.at[me, core], res.at[me, core], s_res.at[k], r_res.at[me], flipped(me, k), core)
    push(res.at[me, core], res.at[me, core], f_res.at[me], b_res.at[me], me, mate)
    for k in reversed(far):
        e = flipped(me, k)
        arrive(res.at[e, core], r_res.at[e])
        push(res.at[e, core], res.at[e, core], f_res.at[e], b_res.at[e], me, mate)
    for k in reversed([*far, 0]):
        e = flipped(me, k)
        arrive(res.at[e, mate], b_res.at[e])
    square = jnp.zeros((rows, 1), jnp.float32)
    for s in range(ep):
        block = res[s].reshape(rows, cols).astype(jnp.float32)
        square = square + jnp.sum(block * block, axis=-1, keepdims=True)
    inv = lax.rsqrt(square / width + RMS_EPS)
    switch = cs[...].astype(jnp.float32)
    gate_sum = jnp.zeros((rows, 1), jnp.float32)
    for s in range(ep):
        at = slice(s * cols, (s + 1) * cols)
        block = res[s].reshape(rows, cols).astype(jnp.float32)
        block = (block * inv * gain2[:, at]).astype(jnp.bfloat16)
        ffn[:, at] = block
        block = block.astype(jnp.float32)
        for i in range(cols // 128):
            line = s * (cols // 128) + i
            part_of = block[:, i * 128 : (i + 1) * 128] * switch[line : line + 1]
            gate_sum = gate_sum + jnp.sum(part_of, axis=-1, keepdims=True)
    branch_scale = 1.0 / (1.0 + jnp.exp(-gate_sum))
    for k in far:
        e = flipped(me, k)
        arrive(share.at[e], r_sh.at[e])
    expert = (me * tp + core) * wg.shape[1] // expert_cols
    table = share[...].astype(jnp.float32).reshape(rows, 128)
    picked = lax.broadcasted_iota(jnp.int32, (rows, 128), 1) == expert
    weight = jnp.sum(jnp.where(picked, table, 0.0), axis=-1, keepdims=True)
    for copy in weights[4:6]:
        copy.wait()

    def widen_up(c, _):
        at = pl.ds(pl.multiple_of(c * 256, 256), 256)
        g = jnp.dot(ffn[...], wg[:, at], preferred_element_type=jnp.float32)
        u = jnp.dot(ffn[...], wu[:, at], preferred_element_type=jnp.float32)
        hid[:, at] = (g / (1.0 + jnp.exp(-g)) * u).astype(jnp.bfloat16)
        return _

    lax.fori_loop(0, wg.shape[1] // 256, widen_up, 0)
    for copy in weights[6:8]:
        copy.wait()
    g, u = across_dot(ffn[...], cg[...]), across_dot(ffn[...], cu[...])
    chid[...] = (g / (1.0 + jnp.exp(-g)) * u).astype(jnp.bfloat16)
    for copy in weights[8:]:
        copy.wait()
    pieces = mine.shape[0]
    piece = width // pieces
    last = own // tp
    for n in range(pieces):
        at = slice(n * piece, (n + 1) * piece)
        y = weight * jnp.dot(hid[...], wd[:, at], preferred_element_type=jnp.float32)
        y = y + branch_scale * jnp.dot(chid[...], cd[:, at], preferred_element_type=jnp.float32)
        y = y.reshape(ep, tp, last, piece)
        for i in range(tp):
            sibout[n, i] = y[:, i].astype(jnp.bfloat16)
        push(sibout.at[n, mate], sibin.at[n], s_sib.at[n], r_sib.at[n], me, mate)
    for n in range(pieces):
        arrive(sibin.at[n], r_sib.at[n])
        mine[n] = (
            sibout[n, core].astype(jnp.float32) + sibin[n].astype(jnp.float32)
        ).astype(jnp.bfloat16)
        for k in far:
            e = flipped(me, k)
            push(mine.at[n, e], got.at[n, me], s_out.at[n, k], r_out.at[n, me], e, core)
    start = pl.multiple_of(lax.rem(me, group) * own, own)
    per = piece // cols
    for n in range(pieces):
        total = mine[n, me].astype(jnp.float32)
        for k in reversed(far):
            e = flipped(me, k)
            arrive(got.at[n, e], r_out.at[n, e])
            total = total + got[n, e].astype(jnp.float32)
        for s in range(per):
            base = res[n * per + s, side, pl.ds(start, own)].astype(jnp.float32)
            base = jnp.where(core == 0, base[:last], base[last:])
            a = n * piece + s * cols
            out[:, a : a + cols] = (base + total[:, s * cols : (s + 1) * cols]).astype(jnp.bfloat16)
    for send in sends:
        send.wait_send()

    @pl.when(jnp.logical_not(here))
    def _():
        across.wait_send()

    @pl.when(here)
    def _():
        for copy in blocks:
            copy.wait_send()


def layer(*blocks):
    own = blocks[0].shape[0]
    cols, hidden = blocks[9].shape[1], blocks[18].shape[1]
    heads = blocks[17].shape[0]
    tiles = cols % 128 == 0 and hidden % 256 == 0 and own % 16 == 0
    tiles = tiles and heads % 8 == 0 and 128 % heads == 0 and heads <= 32
    tiles = tiles and blocks[0].shape[1] % 2048 == 0 and cols % 256 == 0
    ep = lax.axis_size("ep")
    heads_match = ep & (ep - 1) == 0 and ep % 2 == 0 and lax.axis_size("tp") == 2
    weights = sum(2 * w.size for w in blocks[18:24])
    rows = own * ep
    held = weights + rows * (12 * blocks[0].shape[1] + 8 * hidden) + 14 * blocks[1].size
    small = held < VMEM_ROOM
    return (kernel_body if tiles and heads_match and small else body)(*blocks)


def kernel_body(
    fresh_inputs,
    memory_arrays,
    chosen_specialist,
    chosen_coefficient,
    first_rescale,
    second_rescale,
    receiver_projector,
    address_projector,
    content_projector,
    final_projector,
    forget_narrowing,
    forget_widening,
    forget_bias,
    learning_narrowing,
    learning_widening,
    learning_bias,
    lane_scaling,
    instant_reward,
    specialist_switch,
    specialist_expand,
    specialist_contract,
    common_activator,
    common_expand,
    common_contract,
    common_switch,
):
    ep, tp = lax.axis_size("ep"), lax.axis_size("tp")
    own, width = fresh_inputs.shape
    half, cols = width // tp, final_projector.shape[1]
    heads = half // LANE_WIDTH
    group = ep // tp
    vmem = pl.BlockSpec(memory_space=pltpu.VMEM)
    hbm = pl.BlockSpec(memory_space=pl.ANY)
    bf16, f32 = jnp.bfloat16, jnp.float32
    dma = pltpu.SemaphoreType.DMA

    def row(vector):
        return vector.reshape(1, -1)

    rows, hidden, dense = ep * own, specialist_switch.shape[1], common_activator.shape[1]
    low, top = forget_narrowing.shape[1], chosen_specialist.shape[1]
    pack = 4
    wide, block_rows = pack * LANE_WIDTH, heads // pack * LANE_WIDTH
    pieces, batches = 4, 4
    piece, last = width // pieces, own // tp
    per_head = pltpu.VMEM((own, heads, LANE_WIDTH), f32)
    new_tokens, memory_after = pl.pallas_call(
        functools.partial(layer_kernel, ep, tp, FF_E),
        out_shape=(
            pltpu.VMEM((last, width), bf16),
            pltpu.VMEM(memory_arrays.shape, f32),
        ),
        in_specs=[hbm] * 25,
        out_specs=(vmem, vmem),
        scratch_shapes=[
            pltpu.VMEM((own, width), bf16),
            pltpu.VMEM((top, own), jnp.int32),
            pltpu.VMEM((top, own), bf16),
            pltpu.VMEM((1, width), f32),
            pltpu.VMEM((1, width), f32),
            pltpu.VMEM((width // 128, 128), bf16),
            pltpu.VMEM((heads, LANE_WIDTH), f32),
            pltpu.VMEM((1, half), f32),
            pltpu.VMEM((low, width), bf16),
            pltpu.VMEM((low, half), bf16),
            pltpu.VMEM((1, half), f32),
            pltpu.VMEM((low, width), bf16),
            pltpu.VMEM((low, half), bf16),
            pltpu.VMEM((1, half), f32),
            pltpu.VMEM((3, half, cols), bf16),
            pltpu.VMEM((half, cols), bf16),
            pltpu.VMEM((width, hidden), bf16),
            pltpu.VMEM((width, hidden), bf16),
            pltpu.VMEM((hidden, width), bf16),
            pltpu.VMEM((dense, width), bf16),
            pltpu.VMEM((dense, width), bf16),
            pltpu.VMEM((dense, width), bf16),
            pltpu.VMEM((own, block_rows, wide), f32),
            pltpu.VMEM((own, block_rows, wide), bf16),
            pltpu.VMEM((tp, own, half), bf16),
            pltpu.VMEM((ep, own, half), bf16),
            pltpu.VMEM((ep, 3, own, cols), bf16),
            pltpu.VMEM((ep, 3, own, cols), bf16),
            per_head,
            per_head,
            per_head,
            per_head,
            per_head,
            pltpu.VMEM((own, half), f32),
            pltpu.VMEM((heads, LANE_WIDTH), f32),
            pltpu.VMEM((own, 128, LANE_WIDTH), f32),
            pltpu.VMEM((own, 128, wide), bf16),
            pltpu.VMEM((own, 128, wide), bf16),
            pltpu.VMEM((own, block_rows, 128), bf16),
            per_head,
            pltpu.VMEM((own, half), bf16),
            pltpu.VMEM((ep, own, half), bf16),
            pltpu.VMEM((ep, own, cols), bf16),
            pltpu.VMEM((ep, own, 128), bf16),
            pltpu.VMEM((tp, group * own, cols), bf16),
            pltpu.VMEM((group * own, cols), bf16),
            pltpu.VMEM((ep, tp, group * own, cols), bf16),
            pltpu.VMEM((rows, width), bf16),
            pltpu.VMEM((rows, hidden), bf16),
            pltpu.VMEM((rows, dense), bf16),
            pltpu.VMEM((pieces, tp, ep, last, piece), bf16),
            pltpu.VMEM((pieces, ep, last, piece), bf16),
            pltpu.VMEM((pieces, ep, last, piece), bf16),
            pltpu.VMEM((pieces, ep, last, piece), bf16),
            dma((14,)),
            dma((batches,)),
            dma((10,)),
            *[dma((ep,))] * 10,
            dma,
            dma,
            *[dma((ep,))] * 4,
            dma((pieces,)),
            dma((pieces,)),
            dma((pieces, ep)),
            dma((pieces, ep)),
        ],
        compiler_params=pltpu.CompilerParams(
            collective_id=0, has_side_effects=True, vmem_limit_bytes=54 * 2**20
        ),
        name="layer",
    )(
        fresh_inputs,
        memory_arrays,
        chosen_specialist.T,
        chosen_coefficient.T,
        row(first_rescale),
        row(second_rescale),
        common_switch.reshape(-1, 128),
        instant_reward,
        row(lane_scaling),
        receiver_projector,
        address_projector,
        content_projector,
        final_projector,
        forget_narrowing.T,
        forget_widening,
        row(forget_bias),
        learning_narrowing.T,
        learning_widening,
        row(learning_bias),
        specialist_switch,
        specialist_expand,
        specialist_contract,
        common_activator.T,
        common_expand.T,
        common_contract,
    )
    return (new_tokens, memory_after)


def solution(mesh):
    placed = (
        P(("grp", "ep"), None),
        P(("grp", "ep"), "tp", None, None),
        P(("grp", "ep"), None),
        P(("grp", "ep"), None),
        P(),
        P(),
        P("tp", "ep"),
        P("tp", "ep"),
        P("tp", "ep"),
        P("tp", "ep"),
        P(),
        P(None, "tp"),
        P("tp"),
        P(),
        P(None, "tp"),
        P("tp"),
        P("tp"),
        P("tp", None),
        P(None, ("ep", "tp")),
        P(None, ("ep", "tp")),
        P(("ep", "tp"), None),
        P(None, ("ep", "tp")),
        P(None, ("ep", "tp")),
        P(("ep", "tp"), None),
        P(),
    )
    return jax.shard_map(
        layer,
        mesh=mesh,
        in_specs=placed,
        out_specs=(P(("grp", "ep", "tp"), None), P(("grp", "ep"), "tp", None, None)),
        check_vma=False,
    )
```

time: 76.5 us -> 61 us (0.80)
  Pallas kernels: 73.4 us -> 56.1 us
  local copies, waits for them, and re-layouts: 1.98 us -> 4.01 us
    pallas_call x3 -> x1, Pallas kernels: 73.4 us -> 56.1 us  [kernel_body(): pl.pallas_call(functools.partial(layer_kernel, ep, tp, FF_E), out_shape=(...]
    unnamed x3 -> x2, local copies, waits for them, and re-layouts: 1.38 us -> 4.01 us
where the time goes in v1:
time: 61 us; the launch traced here: 60.8 us
  Pallas kernels  56.1 us (92%)
  local copies, waits for them, and re-layouts  4.01 us (7%)
  between operations  0.65 us (1%)
    pallas_call x1, Pallas kernels, kernel_body(): pl.pallas_call(functools.partial(layer_kernel, ep, tp, FF_E), out_shape=(...  56.1 us
    unnamed x2, local copies, waits for them, and re-layouts  4.01 us

profile of v1, /device:TPU:0, one launch (start us, length us, event | category | flops | bytes accessed | tf_op | source)
XLA Modules:
  0.0 60.8 jit_solution(13799666781332987076)
XLA Ops:
  0.6 56.1 %layer.1 = (bf16[8,2048]{1,0:T(8,128)(2,1)S(1)}, f32[16,16,64,64]{3,2,1,0:T(8,128)S(1)}) custom-call(bf16[16,2048]{1,0:T(8,128)(2,1)} %x_h.1, f32[16,16,64,64]{3,2,1,0:T(8,128)} %memory.1, s32[2,16]{1,0:T(2,128)} %bitcast.22, bf16[2,16]{1,0:T(2,128)(2,1)} %bitcast.23, f32[1,2048]{1,0:T(1,128)} %bitcast.16, f32[1,2048]{1,0:T(1,128)} %bitcast.17, ...), custom_call_target="tpu_custom_call" | custom-call | tf_op jit(solution)/shard_map/layer/pallas_call | solution.py:636
  56.8 0.6 %copy.29 = bf16[8,2048]{1,0:T(8,128)(2,1)} copy(bf16[8,2048]{1,0:T(8,128)(2,1)S(1)} %get-tuple-element.2) | data formatting | bytes 65536
  57.4 3.4 %copy.30 = f32[16,16,64,64]{3,2,1,0:T(8,128)} copy(f32[16,16,64,64]{3,2,1,0:T(8,128)S(1)} %get-tuple-element.3) | data formatting | bytes 8388608

commit v2 on v1

--- a/solution.py
+++ b/solution.py
@@ -181,12 +181,12 @@
     return ((own_residual + routed).astype(jnp.bfloat16), memory_after)
 
 
-def flipped(index, mask):
-    for bit in range(mask.bit_length()):
-        step = 1 << bit
-        if mask & step:
-            index = index + step * (1 - 2 * lax.rem(index // step, 2))
-    return index
+def flipped(index, mask, count):
+    total, step = 0, 1
+    while step < count:
+        total = total + step * lax.rem(index // step + mask // step, 2)
+        step = 2 * step
+    return total
 
 
 def _greet(ep, tp):
@@ -198,7 +198,7 @@
                 pl.semaphore_signal(
                     barrier,
                     inc=1,
-                    device_id={"ep": flipped(me, mask), "tp": lax.rem(core + side, tp)},
+                    device_id={"ep": flipped(me, mask, ep), "tp": lax.rem(core + side, tp)},
                     device_id_type=MESH,
                 )
 
@@ -239,11 +239,11 @@
     wq_h, wk_h, wv_h, wo_h, fnar_h, fwid_h, fbias_h, lnar_h, lwid_h, lbias_h,
     wg_h, wu_h, wd_h, cg_h, cu_h, cd_h,
     out, mem,
-    x, ids, coef, gain, gain2, cs, reward, scaling, fnar, fwid, fbias, lnar, lwid, lbias,
+    x, ids, coef, gain, gain2, cs16, cs, reward, scaling, fnar, fwid, fbias, lnar, lwid, lbias,
     w, wo, wg, wu, wd, cg, cu, cd, pk, pk16,
     halves, rows_all, part, gotp, query, key, value, decay, rate, dch, lane_gain,
     flip, probes, moves, factors, read,
-    att, att_all, xcol, share, pbuf, psib, res, ffn, hid, chid, sibout, sibin, mine, got,
+    att, att_all, xcol, share, pbuf, psib, res, gacc, uacc, cgacc, cuacc, sq, gs, hid, chid, sibout, sibin, mine, got,
     lsem, msem, wsem,
     s_row, r_row, s_part, r_part, s_att, r_att, s_x, r_x, s_sh, r_sh, s_p, r_p,
     s_res, r_res, f_res, b_res, s_sib, r_sib, s_out, r_out,
@@ -260,7 +260,9 @@
     pack = pk.shape[2] // LANE_WIDTH
     packs = heads // pack
     block_rows = packs * LANE_WIDTH
-    far = list(range(ep - 1, 0, -1))
+    far = list(range(1, ep))
+    turn_at, turned_by = ep // 2, ep // 2 + 1
+    direct = [turn_at] + [k for k in far if k not in (turn_at, turned_by)]
     _greet(ep, tp)
 
     smalls = [
@@ -269,7 +271,7 @@
             (
                 (x_h, x), (gain_h, gain), (fnar_h, fnar), (fwid_h, fwid), (fbias_h, fbias),
                 (lnar_h, lnar), (lwid_h, lwid), (lbias_h, lbias), (scaling_h, scaling),
-                (reward_h, reward), (ids_h, ids), (coef_h, coef), (gain2_h, gain2), (cs_h, cs),
+                (reward_h, reward), (ids_h, ids), (coef_h, coef), (gain2_h, gain2), (cs_h, cs16),
             )
         )
     ]
@@ -298,18 +300,33 @@
         sends.append(_remote(*args))
         sends[-1].start()
 
+    def spread_out(block, every, send, recv):
+        for k in direct:
+            push(block, every.at[me], send.at[k], recv.at[me], flipped(me, k, ep), core)
+
+    def hand_on(every, send, recv):
+        e = flipped(me, turn_at, ep)
+        arrive(every.at[e], recv.at[e])
+        push(every.at[e], every.at[e], send.at[turned_by], recv.at[e], flipped(me, 1, ep), core)
+
+    def gathered(every, recv):
+        for k in far:
+            if k != turn_at:
+                e = flipped(me, k, ep)
+                arrive(every.at[e], recv.at[e])
+
     for copy in smalls[:2]:
         copy.wait()
     normed = rms_norm(x[...].astype(jnp.float32), gain[...]).astype(jnp.bfloat16)
     for i in range(tp):
         halves[i] = normed[:, i * half : (i + 1) * half]
     _met(ep, tp)
-    for k in far:
-        push(halves.at[core], rows_all.at[me], s_row.at[k], r_row.at[me], flipped(me, k), core)
+    spread_out(halves.at[core], rows_all, s_row, r_row)
     rows_all[me] = halves[core]
 
     for copy in smalls[2:]:
         copy.wait()
+    cs[...] = cs16[...].astype(jnp.float32)
     decay_mid = jnp.tanh(across_dot(normed, fnar[...])).astype(jnp.bfloat16)
     decay_pre = fbias[...] + jnp.dot(decay_mid, fwid[...], preferred_element_type=jnp.float32)
     kept = jnp.exp(-(math.exp(-0.5) / (1.0 + jnp.exp(-decay_pre))))
@@ -331,6 +348,7 @@
         )
     share[me] = routes.astype(jnp.bfloat16)
     xcol[me] = x[:, pl.ds(pl.multiple_of(me * cols, cols), cols)]
+    hand_on(rows_all, s_row, r_row)
     for copy in states:
         copy.wait()
     for copy in weights[3:]:
@@ -348,16 +366,14 @@
 
     for copy in weights[:3]:
         copy.wait()
-    for k in far:
-        e = flipped(me, k)
-        arrive(rows_all.at[e], r_row.at[e])
+    gathered(rows_all, r_row)
     every = rows_all[...].reshape(rows, half)
     for i in range(3):
         done = jnp.dot(every, w[i], preferred_element_type=jnp.float32)
         part[:, i] = done.astype(jnp.bfloat16).reshape(ep, own, cols)
     slot = core * group + lax.rem(me, group)
     for k in far:
-        e = flipped(me, k)
+        e = flipped(me, k, ep)
         push(part.at[e], gotp.at[slot], s_part.at[k], r_part.at[slot], e, side)
     here = side == core
     local = pltpu.make_async_copy(part.at[me], gotp.at[slot], r_part.at[slot])
@@ -373,7 +389,7 @@
 
     blocks = []
     for k in far:
-        e = flipped(me, k)
+        e = flipped(me, k, ep)
         block = x.at[:, pl.ds(pl.multiple_of(e * cols, cols), cols)]
         blocks.append(_remote(block, xcol.at[me], s_x.at[k], r_x.at[me], e, core))
 
@@ -383,7 +399,7 @@
             copy.start()
 
     for k in far:
-        push(share.at[me], share.at[me], s_sh.at[k], r_sh.at[me], flipped(me, k), core)
+        push(share.at[me], share.at[me], s_sh.at[k], r_sh.at[me], flipped(me, k, ep), core)
 
     for j in range(group):
         for s in range(tp):
@@ -438,8 +454,7 @@
     for h in range(0, heads, 2):
         joined = jnp.concatenate([read[:, h + i, :] for i in range(2)], axis=-1)
         att[:, h * LANE_WIDTH : (h + 2) * LANE_WIDTH] = joined.astype(jnp.bfloat16)
-    for k in far:
-        push(att, att_all.at[me], s_att.at[k], r_att.at[me], flipped(me, k), core)
+    spread_out(att, att_all, s_att, r_att)
     att_all[me] = att[...]
 
     def renew(b, _):
@@ -451,12 +466,15 @@
                 mem[b, p * pack + i] = new[:, i * LANE_WIDTH : (i + 1) * LANE_WIDTH]
         return _
 
-    lax.fori_loop(0, own, renew, 0)
+    lax.fori_loop(0, own // 2, renew, 0)
+    hand_on(att_all, s_att, r_att)
+    lax.fori_loop(own // 2, own, renew, 0)
 
     weights[3].wait()
     for k in far:
-        e = flipped(me, k)
-        arrive(att_all.at[e], r_att.at[e])
+        e = flipped(me, k, ep)
+        arrive(share.at[e], r_sh.at[e])
+    gathered(att_all, r_att)
     done = jnp.dot(
         att_all[...].reshape(rows, half), wo[...], preferred_element_type=jnp.float32
     ).astype(jnp.bfloat16)
@@ -473,61 +491,74 @@
     mixed = (pbuf[core].astype(jnp.float32) + psib[...].astype(jnp.float32)).astype(jnp.bfloat16)
     held = xcol[pl.ds(core * group, group)].reshape(group * own, cols).astype(jnp.float32)
     res[me, core] = (held + mixed.astype(jnp.float32)).astype(jnp.bfloat16)
-    for k in far:
-        push(res.at[me, core], res.at[me, core], s_res.at[k], r_res.at[me], flipped(me, k), core)
-    push(res.at[me, core], res.at[me, core], f_res.at[me], b_res.at[me], me, mate)
-    for k in reversed(far):
-        e = flipped(me, k)
+    for k in direct:
+        push(res.at[me, core], res.at[me, core], s_res.at[k], r_res.at[me], flipped(me, k, ep), core)
+    _remote(res.at[me, core], res.at[me, core], f_res.at[me], b_res.at[me], me, mate).start()
+    for ref in (gacc, uacc, cgacc, cuacc, sq, gs):
+        ref[...] = jnp.zeros_like(ref)
+    for copy in weights[4:8]:
+        copy.wait()
+
+    def forward(e):
+        return _remote(res.at[e, core], res.at[e, core], f_res.at[e], b_res.at[e], me, mate)
+
+    def absorb(e):
+        arrive(res.at[e, mate], b_res.at[e])
+        at = pl.ds(pl.multiple_of(e * cols, cols), cols)
+        block = res[e].reshape(rows, cols).astype(jnp.float32)
+        scaled = (block * gain2[:, at]).astype(jnp.bfloat16)
+        gacc[...] += jnp.dot(scaled, wg[at, :], preferred_element_type=jnp.float32)
+        uacc[...] += jnp.dot(scaled, wu[at, :], preferred_element_type=jnp.float32)
+        cgacc[...] += across_dot(scaled, cg[:, at])
+        cuacc[...] += across_dot(scaled, cu[:, at])
+        wide_rows = scaled.astype(jnp.float32)
+        for i in range(cols // 128):
+            part_of = block[:, i * 128 : (i + 1) * 128]
+            sq[...] += part_of * part_of
+            line = cs[pl.ds(e * (cols // 128) + i, 1), :]
+            gs[...] += wide_rows[:, i * 128 : (i + 1) * 128] * line
+
+    ready = me
+    for k in (1, turn_at, *[k for k in range(2, ep) if k not in (turn_at, turned_by)], turned_by):
+        e = flipped(me, k, ep)
         arrive(res.at[e, core], r_res.at[e])
-        push(res.at[e, core], res.at[e, core], f_res.at[e], b_res.at[e], me, mate)
-    for k in reversed([*far, 0]):
-        e = flipped(me, k)
-        arrive(res.at[e, mate], b_res.at[e])
-    square = jnp.zeros((rows, 1), jnp.float32)
-    for s in range(ep):
-        block = res[s].reshape(rows, cols).astype(jnp.float32)
-        square = square + jnp.sum(block * block, axis=-1, keepdims=True)
-    inv = lax.rsqrt(square / width + RMS_EPS)
-    switch = cs[...].astype(jnp.float32)
-    gate_sum = jnp.zeros((rows, 1), jnp.float32)
-    for s in range(ep):
-        at = slice(s * cols, (s + 1) * cols)
-        block = res[s].reshape(rows, cols).astype(jnp.float32)
-        block = (block * inv * gain2[:, at]).astype(jnp.bfloat16)
-        ffn[:, at] = block
-        block = block.astype(jnp.float32)
-        for i in range(cols // 128):
-            line = s * (cols // 128) + i
-            part_of = block[:, i * 128 : (i + 1) * 128] * switch[line : line + 1]
-            gate_sum = gate_sum + jnp.sum(part_of, axis=-1, keepdims=True)
-    branch_scale = 1.0 / (1.0 + jnp.exp(-gate_sum))
-    for k in far:
-        e = flipped(me, k)
-        arrive(share.at[e], r_sh.at[e])
+        if k == turn_at:
+            push(
+                res.at[e, core], res.at[e, core], s_res.at[turned_by], r_res.at[e],
+                flipped(me, 1, ep), core,
+            )
+        forward(e).start()
+        absorb(ready)
+        ready = e
+    absorb(ready)
+    inv = lax.rsqrt(jnp.sum(sq[...], axis=-1, keepdims=True) / width + RMS_EPS)
+    branch_scale = 1.0 / (1.0 + jnp.exp(-inv * jnp.sum(gs[...], axis=-1, keepdims=True)))
     expert = (me * tp + core) * wg.shape[1] // expert_cols
     table = share[...].astype(jnp.float32).reshape(rows, 128)
     picked = lax.broadcasted_iota(jnp.int32, (rows, 128), 1) == expert
     weight = jnp.sum(jnp.where(picked, table, 0.0), axis=-1, keepdims=True)
-    for copy in weights[4:6]:
-        copy.wait()
-
-    def widen_up(c, _):
-        at = pl.ds(pl.multiple_of(c * 256, 256), 256)
-        g = jnp.dot(ffn[...], wg[:, at], preferred_element_type=jnp.float32)
-        u = jnp.dot(ffn[...], wu[:, at], preferred_element_type=jnp.float32)
-        hid[:, at] = (g / (1.0 + jnp.exp(-g)) * u).astype(jnp.bfloat16)
-        return _
-
-    lax.fori_loop(0, wg.shape[1] // 256, widen_up, 0)
-    for copy in weights[6:8]:
-        copy.wait()
-    g, u = across_dot(ffn[...], cg[...]), across_dot(ffn[...], cu[...])
-    chid[...] = (g / (1.0 + jnp.exp(-g)) * u).astype(jnp.bfloat16)
+
+    def gated(target, gates, ups):
+        g, u = gates[...] * inv, ups[...] * inv
+        target[...] = (g / (1.0 + jnp.exp(-g)) * u).astype(jnp.bfloat16)
+
+    gated(hid, gacc, uacc)
+    gated(chid, cgacc, cuacc)
     for copy in weights[8:]:
         copy.wait()
     pieces = mine.shape[0]
     piece = width // pieces
     last = own // tp
+
+    def finish(n):
+        arrive(sibin.at[n], r_sib.at[n])
+        mine[n] = (
+            sibout[n, core].astype(jnp.float32) + sibin[n].astype(jnp.float32)
+        ).astype(jnp.bfloat16)
+        for k in far:
+            e = flipped(me, k, ep)
+            push(mine.at[n, e], got.at[n, me], s_out.at[n, k], r_out.at[n, me], e, core)
+
     for n in range(pieces):
         at = slice(n * piece, (n + 1) * piece)
         y = weight * jnp.dot(hid[...], wd[:, at], preferred_element_type=jnp.float32)
@@ -536,20 +567,15 @@
         for i in range(tp):
             sibout[n, i] = y[:, i].astype(jnp.bfloat16)
         push(sibout.at[n, mate], sibin.at[n], s_sib.at[n], r_sib.at[n], me, mate)
-    for n in range(pieces):
-        arrive(sibin.at[n], r_sib.at[n])
-        mine[n] = (
-            sibout[n, core].astype(jnp.float32) + sibin[n].astype(jnp.float32)
-        ).astype(jnp.bfloat16)
-        for k in far:
-            e = flipped(me, k)
-            push(mine.at[n, e], got.at[n, me], s_out.at[n, k], r_out.at[n, me], e, core)
+        if n:
+            finish(n - 1)
+    finish(pieces - 1)
     start = pl.multiple_of(lax.rem(me, group) * own, own)
     per = piece // cols
     for n in range(pieces):
         total = mine[n, me].astype(jnp.float32)
         for k in reversed(far):
-            e = flipped(me, k)
+            e = flipped(me, k, ep)
             arrive(got.at[n, e], r_out.at[n, e])
             total = total + got[n, e].astype(jnp.float32)
         for s in range(per):
@@ -559,6 +585,8 @@
             out[:, a : a + cols] = (base + total[:, s * cols : (s + 1) * cols]).astype(jnp.bfloat16)
     for send in sends:
         send.wait_send()
+    for e in range(ep):
+        forward(e).wait_send()
 
     @pl.when(jnp.logical_not(here))
     def _():
@@ -568,6 +596,18 @@
     def _():
         for copy in blocks:
             copy.wait_send()
+
+
+def settle_kernel(tokens, state, out, after, sems):
+    step = state.shape[0] // (sems.shape[0] - 1)
+    copies = [pltpu.make_async_copy(tokens, out, sems.at[0])]
+    for i in range(sems.shape[0] - 1):
+        at = pl.ds(i * step, step)
+        copies.append(pltpu.make_async_copy(state.at[at], after.at[at], sems.at[i + 1]))
+    for copy in copies:
+        copy.start()
+    for copy in copies:
+        copy.wait()
 
 
 def layer(*blocks):
@@ -578,7 +618,7 @@
     tiles = tiles and heads % 8 == 0 and 128 % heads == 0 and heads <= 32
     tiles = tiles and blocks[0].shape[1] % 2048 == 0 and cols % 256 == 0
     ep = lax.axis_size("ep")
-    heads_match = ep & (ep - 1) == 0 and ep % 2 == 0 and lax.axis_size("tp") == 2
+    heads_match = ep & (ep - 1) == 0 and ep > 2 and lax.axis_size("tp") == 2
     weights = sum(2 * w.size for w in blocks[18:24])
     rows = own * ep
     held = weights + rows * (12 * blocks[0].shape[1] + 8 * hidden) + 14 * blocks[1].size
@@ -648,6 +688,7 @@
             pltpu.VMEM((1, width), f32),
             pltpu.VMEM((1, width), f32),
             pltpu.VMEM((width // 128, 128), bf16),
+            pltpu.VMEM((width // 128, 128), f32),
             pltpu.VMEM((heads, LANE_WIDTH), f32),
             pltpu.VMEM((1, half), f32),
             pltpu.VMEM((low, width), bf16),
@@ -689,7 +730,12 @@
             pltpu.VMEM((tp, group * own, cols), bf16),
             pltpu.VMEM((group * own, cols), bf16),
             pltpu.VMEM((ep, tp, group * own, cols), bf16),
-            pltpu.VMEM((rows, width), bf16),
+            pltpu.VMEM((rows, hidden), f32),
+            pltpu.VMEM((rows, hidden), f32),
+            pltpu.VMEM((rows, dense), f32),
+            pltpu.VMEM((rows, dense), f32),
+            pltpu.VMEM((rows, 128), f32),
+            pltpu.VMEM((rows, 128), f32),
             pltpu.VMEM((rows, hidden), bf16),
             pltpu.VMEM((rows, dense), bf16),
             pltpu.VMEM((pieces, tp, ep, last, piece), bf16),
@@ -739,7 +785,21 @@
         common_expand.T,
         common_contract,
     )
-    return (new_tokens, memory_after)
+    return pl.pallas_call(
+        settle_kernel,
+        out_shape=(
+            jax.ShapeDtypeStruct((last, width), bf16),
+            jax.ShapeDtypeStruct(memory_arrays.shape, f32),
+        ),
+        in_specs=[vmem] * 2,
+        out_specs=(hbm,) * 2,
+        scratch_shapes=[dma((5,))],
+        compiler_params=pltpu.CompilerParams(vmem_limit_bytes=2**20),
+        name="settle",
+    )(
+        pltpu.with_memory_space_constraint(new_tokens, pltpu.VMEM),
+        pltpu.with_memory_space_constraint(memory_after, pltpu.VMEM),
+    )
 
 
 def solution(mesh):

time: 61 us -> 54.7 us (0.90)
  local copies, waits for them, and re-layouts: 4.01 us -> 0 us
  Pallas kernels: 56.1 us -> 53.9 us
    pallas_call x1, Pallas kernels: 56.1 us -> 50.6 us  [kernel_body(): pl.pallas_call(functools.partial(layer_kernel, ep, tp, FF_E), out_shape=(...]
    unnamed x2 -> x0, local copies, waits for them, and re-layouts: 4.01 us -> none
    pallas_call x0 -> x1, Pallas kernels: none -> 3.39 us  [kernel_body(): pl.pallas_call(settle_kernel, out_shape=(jax.ShapeDtypeStruct((last, widt...]
where the time goes in v2:
time: 54.7 us; the launch traced here: 54.6 us
  Pallas kernels  53.9 us (99%)
  between operations  0.65 us (1%)
    pallas_call x1, Pallas kernels, kernel_body(): pl.pallas_call(functools.partial(layer_kernel, ep, tp, FF_E), out_shape=(...  50.6 us
    pallas_call x1, Pallas kernels, kernel_body(): pl.pallas_call(settle_kernel, out_shape=(jax.ShapeDtypeStruct((last, widt...  3.39 us

profile of v2, /device:TPU:0, one launch (start us, length us, event | category | flops | bytes accessed | tf_op | source)
XLA Modules:
  0.0 54.6 jit_solution(14094646785056293225)
XLA Ops:
  0.6 50.6 %layer.1 = (bf16[8,2048]{1,0:T(8,128)(2,1)S(1)}, f32[16,16,64,64]{3,2,1,0:T(8,128)S(1)}) custom-call(bf16[16,2048]{1,0:T(8,128)(2,1)} %x_h.1, f32[16,16,64,64]{3,2,1,0:T(8,128)} %memory.1, s32[2,16]{1,0:T(2,128)} %bitcast.22, bf16[2,16]{1,0:T(2,128)(2,1)} %bitcast.23, f32[1,2048]{1,0:T(1,128)} %bitcast.16, f32[1,2048]{1,0:T(1,128)} %bitcast.17, ...), custom_call_target="tpu_custom_call" | custom-call | tf_op jit(solution)/shard_map/layer/pallas_call | solution.py:676
  51.2 3.4 %settle.1 = (bf16[8,2048]{1,0:T(8,128)(2,1)}, f32[16,16,64,64]{3,2,1,0:T(8,128)}) custom-call(bf16[8,2048]{1,0:T(8,128)(2,1)S(1)} %get-tuple-element.4.tokens, f32[16,16,64,64]{3,2,1,0:T(8,128)S(1)} %get-tuple-element.5.state), custom_call_target="tpu_custom_call" | custom-call | tf_op jit(solution)/shard_map/settle/pallas_call | solution.py:788

commit v3 on v2

--- a/solution.py
+++ b/solution.py
@@ -224,11 +224,6 @@
     )
 
 
-def by_head(ref, channels, first):
-    for h in range(channels.shape[1] // LANE_WIDTH):
-        ref[:, first + h, :] = channels[:, h * LANE_WIDTH : (h + 1) * LANE_WIDTH]
-
-
 def arrive(ref, sem):
     pltpu.make_async_copy(ref, ref, sem).wait()
 
@@ -239,15 +234,18 @@
     wq_h, wk_h, wv_h, wo_h, fnar_h, fwid_h, fbias_h, lnar_h, lwid_h, lbias_h,
     wg_h, wu_h, wd_h, cg_h, cu_h, cd_h,
     out, mem,
-    x, ids, coef, gain, gain2, cs16, cs, reward, scaling, fnar, fwid, fbias, lnar, lwid, lbias,
-    w, wo, wg, wu, wd, cg, cu, cd, pk, pk16,
-    halves, rows_all, part, gotp, query, key, value, decay, rate, dch, lane_gain,
-    flip, probes, moves, factors, read,
-    att, att_all, xcol, share, pbuf, psib, res, gacc, uacc, cgacc, cuacc, sq, gs, hid, chid, sibout, sibin, mine, got,
+    x, ids, coef, gains, cs16, cs, reward, rows_in, narrow, widen_w,
+    w, wo, wgu, wd, cgu, cd, pk, pk16,
+    halves, rows_all, part, gotp, dch, rch, wch, same, pick,
+    moves, factors, att, att_all, xcol, share, pbuf, psib, res,
+    gacc, uacc, cgacc, cuacc, sq, gs, hid, chid, sibout, sibin, mine, got,
     lsem, msem, wsem,
-    s_row, r_row, s_part, r_part, s_att, r_att, s_x, r_x, s_sh, r_sh, s_p, r_p,
-    s_res, r_res, f_res, b_res, s_sib, r_sib, s_out, r_out,
+    s_row, r_row, t_row, s_part, a_part, r_part, s_att, r_att, t_att, s_x, r_x, s_sh, r_sh,
+    s_p, r_p, s_res, r_res, f_res, b_res, s_sib, r_sib, s_out, r_out,
 ):
+    gain, gain2 = gains.at[0], gains.at[1]
+    fbias, lbias, scaling = rows_in.at[0], rows_in.at[1], rows_in.at[2]
+    wg, wu, cg, cu = wgu.at[0], wgu.at[1], cgu.at[0], cgu.at[1]
     me, core = lax.axis_index("ep"), lax.axis_index("tp")
     mate = lax.rem(core + 1, tp)
     group = ep // tp
@@ -256,7 +254,7 @@
     half = width // tp
     cols = wo.shape[1]
     rows = ep * own
-    heads = lane_gain.shape[0]
+    heads = half // LANE_WIDTH
     pack = pk.shape[2] // LANE_WIDTH
     packs = heads // pack
     block_rows = packs * LANE_WIDTH
@@ -265,80 +263,78 @@
     direct = [turn_at] + [k for k in far if k not in (turn_at, turned_by)]
     _greet(ep, tp)
 
-    smalls = [
-        pltpu.make_async_copy(a, b, lsem.at[i])
-        for i, (a, b) in enumerate(
-            (
-                (x_h, x), (gain_h, gain), (fnar_h, fnar), (fwid_h, fwid), (fbias_h, fbias),
-                (lnar_h, lnar), (lwid_h, lwid), (lbias_h, lbias), (scaling_h, scaling),
-                (reward_h, reward), (ids_h, ids), (coef_h, coef), (gain2_h, gain2), (cs_h, cs16),
-            )
-        )
-    ]
-    weights = [
-        pltpu.make_async_copy(a, b, wsem.at[i])
-        for i, (a, b) in enumerate(
-            (
-                (wq_h, w.at[0]), (wk_h, w.at[1]), (wv_h, w.at[2]), (wo_h, wo), (wg_h, wg),
-                (wu_h, wu), (cg_h, cg), (cu_h, cu), (wd_h, wd), (cd_h, cd),
-            )
-        )
-    ]
-    batches = msem.shape[0]
+    def load(sem, *pairs):
+        return [pltpu.make_async_copy(a, b, sem) for a, b in pairs]
+
+    batches = 4
     batch = own // batches
+    early = load(lsem.at[0], (x_h, x)) + load(lsem.at[1], (gain_h, gain), (gain2_h, gain2))
+    smalls = (
+        load(lsem.at[2], (fnar_h, narrow.at[0]), (lnar_h, narrow.at[1]))
+        + load(lsem.at[3], (fwid_h, widen_w.at[0]), (lwid_h, widen_w.at[1]))
+        + load(lsem.at[4], (fbias_h, fbias), (lbias_h, lbias), (scaling_h, scaling))
+        + load(lsem.at[5], (reward_h, reward))
+        + load(lsem.at[6], (ids_h, ids))
+        + load(lsem.at[7], (coef_h, coef))
+        + load(lsem.at[8], (cs_h, cs16))
+        + load(wsem.at[0], (wq_h, w.at[0]), (wk_h, w.at[1]), (wv_h, w.at[2]))
+    )
     states = [
         pltpu.make_async_copy(
-            memory.at[pl.ds(i * batch, batch)], mem.at[pl.ds(i * batch, batch)], msem.at[i]
+            memory.at[pl.ds(i * batch, batch)], mem.at[pl.ds(i * batch, batch)], msem
         )
         for i in range(batches)
     ]
-    for copy in smalls + weights[:3] + states:
+    weights = (
+        load(wsem.at[1], (wo_h, wo))
+        + load(wsem.at[2], (wg_h, wg), (wu_h, wu))
+        + load(wsem.at[3], (cg_h, cg), (cu_h, cu))
+        + load(wsem.at[4], (wd_h, wd))
+        + load(wsem.at[5], (cd_h, cd))
+    )
+    for copy in early + smalls + states:
         copy.start()
-    sends = []
 
     def push(*args):
-        sends.append(_remote(*args))
-        sends[-1].start()
-
-    def spread_out(block, every, send, recv):
+        _remote(*args).start()
+
+    def spread_out(block, every, send, recv, turn):
         for k in direct:
-            push(block, every.at[me], send.at[k], recv.at[me], flipped(me, k, ep), core)
-
-    def hand_on(every, send, recv):
+            arrives = turn if k == turn_at else recv
+            push(block, every.at[me], send, arrives, flipped(me, k, ep), core)
+
+    def hand_on(every, send, recv, turn):
         e = flipped(me, turn_at, ep)
-        arrive(every.at[e], recv.at[e])
-        push(every.at[e], every.at[e], send.at[turned_by], recv.at[e], flipped(me, 1, ep), core)
-
-    def gathered(every, recv):
-        for k in far:
-            if k != turn_at:
-                e = flipped(me, k, ep)
-                arrive(every.at[e], recv.at[e])
-
-    for copy in smalls[:2]:
-        copy.wait()
+        arrive(every.at[e], turn)
+        push(every.at[e], every.at[e], send, recv, flipped(me, 1, ep), core)
+
+    arrive(x, lsem.at[0])
+    arrive(gains, lsem.at[1])
     normed = rms_norm(x[...].astype(jnp.float32), gain[...]).astype(jnp.bfloat16)
     for i in range(tp):
         halves[i] = normed[:, i * half : (i + 1) * half]
     _met(ep, tp)
-    spread_out(halves.at[core], rows_all, s_row, r_row)
+    spread_out(halves.at[core], rows_all, s_row, r_row, t_row)
     rows_all[me] = halves[core]
 
-    for copy in smalls[2:]:
-        copy.wait()
+    for ref, at in ((narrow, 2), (widen_w, 3), (rows_in, 4), (reward, 5), (ids, 6), (coef, 7), (cs16, 8)):
+        arrive(ref, lsem.at[at])
     cs[...] = cs16[...].astype(jnp.float32)
-    decay_mid = jnp.tanh(across_dot(normed, fnar[...])).astype(jnp.bfloat16)
-    decay_pre = fbias[...] + jnp.dot(decay_mid, fwid[...], preferred_element_type=jnp.float32)
+    decay_mid = jnp.tanh(across_dot(normed, narrow[0])).astype(jnp.bfloat16)
+    decay_pre = fbias[...] + jnp.dot(decay_mid, widen_w[0], preferred_element_type=jnp.float32)
     kept = jnp.exp(-(math.exp(-0.5) / (1.0 + jnp.exp(-decay_pre))))
     dch[...] = kept
-    by_head(decay, kept, 0)
-    rate_mid = across_dot(normed, lnar[...]).astype(jnp.bfloat16)
-    rate_pre = lbias[...] + jnp.dot(rate_mid, lwid[...], preferred_element_type=jnp.float32)
-    by_head(rate, 1.0 / (1.0 + jnp.exp(-rate_pre)), 0)
+    rate_mid = across_dot(normed, narrow[1]).astype(jnp.bfloat16)
+    rate_pre = lbias[...] + jnp.dot(rate_mid, widen_w[1], preferred_element_type=jnp.float32)
+    rch[...] = 1.0 / (1.0 + jnp.exp(-rate_pre))
     for h in range(heads):
-        lane_gain[h : h + 1] = scaling[:, h * LANE_WIDTH : (h + 1) * LANE_WIDTH]
-    for ref in (flip, probes, moves):
-        ref[...] = jnp.zeros_like(ref)
+        wch[:, h * LANE_WIDTH : (h + 1) * LANE_WIDTH] = reward[h : h + 1]
+    first = lax.broadcasted_iota(jnp.int32, same.shape, 0) // LANE_WIDTH
+    other = lax.broadcasted_iota(jnp.int32, same.shape, 1) // LANE_WIDTH
+    same[...] = jnp.where(first == other, 1.0, 0.0).astype(jnp.bfloat16)
+    line = lax.broadcasted_iota(jnp.int32, (own, pick.shape[2]), 0)
+    for b in range(own):
+        pick[b] = jnp.where(line == b, 1.0, 0.0).astype(jnp.bfloat16)
     lane = lax.broadcasted_iota(jnp.int32, (own, 128), 1)
     routes = jnp.zeros((own, 128), jnp.float32)
     ids_cols, coef_cols = ids[...].T, coef[...].astype(jnp.float32).T
@@ -348,10 +344,9 @@
         )
     share[me] = routes.astype(jnp.bfloat16)
     xcol[me] = x[:, pl.ds(pl.multiple_of(me * cols, cols), cols)]
-    hand_on(rows_all, s_row, r_row)
-    for copy in states:
-        copy.wait()
-    for copy in weights[3:]:
+    hand_on(rows_all, s_row, r_row, t_row)
+    arrive(mem, msem)
+    for copy in weights:
         copy.start()
 
     def join(b, _):
@@ -364,20 +359,20 @@
 
     lax.fori_loop(0, own, join, 0)
 
-    for copy in weights[:3]:
-        copy.wait()
-    gathered(rows_all, r_row)
+    arrive(w, wsem.at[0])
+    arrive(rows_all.at[pl.ds(0, ep - 2)], r_row)
     every = rows_all[...].reshape(rows, half)
     for i in range(3):
         done = jnp.dot(every, w[i], preferred_element_type=jnp.float32)
         part[:, i] = done.astype(jnp.bfloat16).reshape(ep, own, cols)
-    slot = core * group + lax.rem(me, group)
+    place = lax.rem(me, group)
+    slot = core * group + place
     for k in far:
         e = flipped(me, k, ep)
-        push(part.at[e], gotp.at[slot], s_part.at[k], r_part.at[slot], e, side)
+        push(part.at[e], gotp.at[slot], s_part, r_part.at[place], e, side)
     here = side == core
-    local = pltpu.make_async_copy(part.at[me], gotp.at[slot], r_part.at[slot])
-    across = _remote(part.at[me], gotp.at[slot], s_part.at[0], r_part.at[slot], me, side)
+    local = pltpu.make_async_copy(part.at[me], gotp.at[slot], r_part.at[place])
+    across = _remote(part.at[me], gotp.at[slot], a_part, r_part.at[place], me, side)
 
     @pl.when(here)
     def _():
@@ -391,7 +386,7 @@
     for k in far:
         e = flipped(me, k, ep)
         block = x.at[:, pl.ds(pl.multiple_of(e * cols, cols), cols)]
-        blocks.append(_remote(block, xcol.at[me], s_x.at[k], r_x.at[me], e, core))
+        blocks.append(_remote(block, xcol.at[me], s_x, r_x, e, core))
 
     @pl.when(here)
     def _():
@@ -399,108 +394,138 @@
             copy.start()
 
     for k in far:
-        push(share.at[me], share.at[me], s_sh.at[k], r_sh.at[me], flipped(me, k, ep), core)
-
-    for j in range(group):
-        for s in range(tp):
-            arrive(gotp.at[s * group + j], r_part.at[s * group + j])
+        push(share.at[me], share.at[me], s_sh, r_sh, flipped(me, k, ep), core)
+
+    wide = pack * LANE_WIDTH
+    inner = lax.broadcasted_iota(jnp.int32, (own, wide), 1) // LANE_WIDTH
+
+    def within(channels):
+        high = channels.astype(jnp.bfloat16)
+        low = (channels - high.astype(jnp.float32)).astype(jnp.bfloat16)
+        both = jnp.dot(
+            jnp.concatenate([high, low], axis=0), same[...], preferred_element_type=jnp.float32
+        )
+        return both[: channels.shape[0]] + both[channels.shape[0] :]
+
+    def stack(*kinds):
+        return jnp.concatenate(
+            [jnp.where(inner == i, kind, 0.0) for kind in kinds for i in range(pack)], axis=0
+        ).astype(jnp.bfloat16)
+
+    def only(stacked, b):
+        split = stacked.reshape(2 * pack, own, wide) * pick[b][None]
+        return split.reshape(2 * pack * own, wide)
+
+    def lanes_of(lines):
+        return jnp.concatenate(
+            [lines[i * own : (i + 1) * own] for i in range(pack)], axis=-1
+        )
+
+    def rows_of(channels):
+        return jnp.concatenate(
+            [channels[:, i * LANE_WIDTH : (i + 1) * LANE_WIDTH] for i in range(pack)], axis=0
+        )
+
+    def column_of(channels):
+        return jnp.concatenate(
+            [channels[:, i * LANE_WIDTH : i * LANE_WIDTH + 1] for i in range(pack)], axis=0
+        )
+
+    def pass_att(j):
+        hand_on(att_all.at[j], s_att, r_att, t_att.at[j])
+
+    order = [flipped(lax.rem(me, group), j, group) for j in range(packs)]
+    for turn, j in enumerate(order):
+        arrive(gotp.at[pl.ds(0, tp)], r_part.at[j])
+        sums = []
         for i in range(3):
             total = gotp[j, i].astype(jnp.float32)
             for s in range(1, tp):
                 total = total + gotp[s * group + j, i].astype(jnp.float32)
-            total = total.astype(jnp.bfloat16).astype(jnp.float32)
-            by_head((query, key, value)[i], total, j * (cols // LANE_WIDTH))
-
-    wide = pack * LANE_WIDTH
-    placed = lax.rem(
-        lax.broadcasted_iota(jnp.int32, (heads, wide), 0), pack
-    ) == lax.broadcasted_iota(jnp.int32, (heads, wide), 1) // LANE_WIDTH
-    vlane = lax.broadcasted_iota(jnp.int32, (LANE_WIDTH, 128), 1)
-    turn = lax.rem(vlane, heads) // pack
-
-    def spread(channels):
-        return jnp.where(placed, jnp.concatenate([channels] * pack, axis=-1), 0.0).astype(
-            jnp.bfloat16
+            sums.append(total.astype(jnp.bfloat16).astype(jnp.float32))
+        q, k, v = sums
+        at = pl.ds(pl.multiple_of(j * wide, wide), wide)
+        down = pl.ds(pl.multiple_of(j * LANE_WIDTH, LANE_WIDTH), LANE_WIDTH)
+        r = rch[:, at]
+        scaled = k * r
+        met = scaled * q
+        sizes = within(jnp.concatenate([k * k, met, met * wch[:, at]], axis=0))
+        inverse = lax.rsqrt(sizes[:own] + 1.0)
+        unit = k * inverse
+        stacked = stack(unit, dch[:, at] * q)
+        v_rows = rows_of(v)
+        acc = jnp.zeros((128, LANE_WIDTH), jnp.float32)
+        for b in range(own):
+            acc = acc + across_dot(only(stacked, b), pk16[b, down])
+        key_met = sizes[own : 2 * own]
+        seen = (
+            acc[pack * own :]
+            - acc[: pack * own] * column_of(inverse * key_met)
+            + v_rows * column_of(key_met)
         )
-
-    for b in range(own):
-        q, k, v, r = query[b], key[b], value[b], rate[b]
-        unit = k * lax.rsqrt(jnp.sum(k * k, axis=-1, keepdims=True) + 1.0)
-        scaled, pulled, seen = k * r, unit * r, decay[b] * q
-        flip[b, 2 * heads : 3 * heads] = v
-        probes[b, 0:heads] = spread(unit)
-        probes[b, heads : 2 * heads] = spread(seen)
-        moves[b, 0:heads] = spread(-pulled)
-        moves[b, 2 * heads : 3 * heads] = spread(scaled)
-        value_cols = flip[b].T
-        sums = across_dot(pk16[b], probes[b])
-        found = jnp.zeros((LANE_WIDTH, 128), jnp.float32)
+        centred = seen - jnp.mean(seen, axis=-1, keepdims=True)
+        level = lax.rsqrt(jnp.mean(centred * centred, axis=-1, keepdims=True) + GROUP_EPS)
+        att[j] = (
+            lanes_of(centred * level) * scaling[:, at] + sizes[2 * own :] * v
+        ).astype(jnp.bfloat16)
+        spread_out(att.at[j], att_all.at[j], s_att, r_att, t_att.at[j])
+        att_all[j, me] = att[j]
+        factors[j] = (
+            jnp.concatenate([acc[: pack * own], v_rows], axis=0).T.astype(jnp.bfloat16)
+        )
+        moves[j] = stack(-(unit * r), scaled)
+        if turn > 2:
+            pass_att(order[turn - 3])
+    def renew(b, _):
         for p in range(packs):
+            change = jnp.dot(factors[p], only(moves[p], b), preferred_element_type=jnp.float32)
             at = slice(p * LANE_WIDTH, (p + 1) * LANE_WIDTH)
-            both = jnp.where(vlane < 2 * heads, sums[at], value_cols)
-            both = jnp.where(turn == p, both, 0.0)
-            factors[b, at] = both.astype(jnp.bfloat16)
-            found = found + both
-        turned = found.T
-        seen_rows = (
-            turned[heads : 2 * heads]
-            - turned[0:heads] * jnp.sum(pulled * q, axis=-1, keepdims=True)
-            + v * jnp.sum(scaled * q, axis=-1, keepdims=True)
-        )
-        centred = seen_rows - jnp.mean(seen_rows, axis=-1, keepdims=True)
-        level = lax.rsqrt(jnp.mean(centred * centred, axis=-1, keepdims=True) + GROUP_EPS)
-        extra = jnp.sum(q * scaled * reward[...], axis=-1, keepdims=True) * v
-        read[b] = centred * level * lane_gain[...] + extra
-    for h in range(0, heads, 2):
-        joined = jnp.concatenate([read[:, h + i, :] for i in range(2)], axis=-1)
-        att[:, h * LANE_WIDTH : (h + 2) * LANE_WIDTH] = joined.astype(jnp.bfloat16)
-    spread_out(att, att_all, s_att, r_att)
-    att_all[me] = att[...]
-
-    def renew(b, _):
-        change = jnp.dot(factors[b], moves[b], preferred_element_type=jnp.float32)
-        for p in range(packs):
-            at = slice(p * LANE_WIDTH, (p + 1) * LANE_WIDTH)
-            new = pk[b, at] * dch[pl.ds(b, 1), p * wide : (p + 1) * wide] + change[at]
+            new = pk[b, at] * dch[pl.ds(b, 1), p * wide : (p + 1) * wide] + change
             for i in range(pack):
                 mem[b, p * pack + i] = new[:, i * LANE_WIDTH : (i + 1) * LANE_WIDTH]
         return _
 
-    lax.fori_loop(0, own // 2, renew, 0)
-    hand_on(att_all, s_att, r_att)
-    lax.fori_loop(own // 2, own, renew, 0)
-
-    weights[3].wait()
-    for k in far:
-        e = flipped(me, k, ep)
-        arrive(share.at[e], r_sh.at[e])
-    gathered(att_all, r_att)
-    done = jnp.dot(
-        att_all[...].reshape(rows, half), wo[...], preferred_element_type=jnp.float32
-    ).astype(jnp.bfloat16)
+    eighth = own // 8
+    for turn in range(1, packs):
+        lax.fori_loop((turn - 1) * eighth, turn * eighth, renew, 0)
+        pass_att(order[turn])
+    lax.fori_loop((packs - 1) * eighth, own // 2, renew, 0)
+    arrive(wo, wsem.at[1])
+    arrive(share.at[pl.ds(0, ep - 1)], r_sh)
+    arrive(att_all.at[:, pl.ds(0, ep - 2)], r_att)
+    done = jnp.zeros((rows, cols), jnp.float32)
+    for j in range(packs):
+        done = done + jnp.dot(
+            att_all[j].reshape(rows, wide),
+            wo[j * wide : (j + 1) * wide],
+            preferred_element_type=jnp.float32,
+        )
+    done = done.astype(jnp.bfloat16)
     pbuf[...] = done.reshape(tp, group * own, cols)
     push(pbuf.at[mate], psib, s_p, r_p, me, mate)
-    for j in range(group):
-        e = core * group + j
-
-        @pl.when(e != me)
-        def _():
-            arrive(xcol.at[e], r_x.at[e])
+
+    @pl.when(here)
+    def _():
+        arrive(xcol.at[pl.ds(0, group - 1)], r_x)
+
+    @pl.when(jnp.logical_not(here))
+    def _():
+        arrive(xcol.at[pl.ds(0, group)], r_x)
 
     arrive(psib, r_p)
     mixed = (pbuf[core].astype(jnp.float32) + psib[...].astype(jnp.float32)).astype(jnp.bfloat16)
     held = xcol[pl.ds(core * group, group)].reshape(group * own, cols).astype(jnp.float32)
     res[me, core] = (held + mixed.astype(jnp.float32)).astype(jnp.bfloat16)
     for k in direct:
-        push(res.at[me, core], res.at[me, core], s_res.at[k], r_res.at[me], flipped(me, k, ep), core)
-    _remote(res.at[me, core], res.at[me, core], f_res.at[me], b_res.at[me], me, mate).start()
+        push(res.at[me, core], res.at[me, core], s_res, r_res.at[me], flipped(me, k, ep), core)
+    push(res.at[me, core], res.at[me, core], f_res, b_res.at[me], me, mate)
     for ref in (gacc, uacc, cgacc, cuacc, sq, gs):
         ref[...] = jnp.zeros_like(ref)
-    for copy in weights[4:8]:
-        copy.wait()
+    arrive(wgu, wsem.at[2])
+    arrive(cgu, wsem.at[3])
 
     def forward(e):
-        return _remote(res.at[e, core], res.at[e, core], f_res.at[e], b_res.at[e], me, mate)
+        push(res.at[e, core], res.at[e, core], f_res, b_res.at[e], me, mate)
 
     def absorb(e):
         arrive(res.at[e, mate], b_res.at[e])
@@ -519,15 +544,15 @@
             gs[...] += wide_rows[:, i * 128 : (i + 1) * 128] * line
 
     ready = me
-    for k in (1, turn_at, *[k for k in range(2, ep) if k not in (turn_at, turned_by)], turned_by):
+    for k in (1, 2, turn_at, *[k for k in range(3, ep) if k not in (turn_at, turned_by)], turned_by):
         e = flipped(me, k, ep)
         arrive(res.at[e, core], r_res.at[e])
         if k == turn_at:
             push(
-                res.at[e, core], res.at[e, core], s_res.at[turned_by], r_res.at[e],
+                res.at[e, core], res.at[e, core], s_res, r_res.at[e],
                 flipped(me, 1, ep), core,
             )
-        forward(e).start()
+        forward(e)
         absorb(ready)
         ready = e
     absorb(ready)
@@ -544,8 +569,8 @@
 
     gated(hid, gacc, uacc)
     gated(chid, cgacc, cuacc)
-    for copy in weights[8:]:
-        copy.wait()
+    arrive(wd, wsem.at[4])
+    arrive(cd, wsem.at[5])
     pieces = mine.shape[0]
     piece = width // pieces
     last = own // tp
@@ -557,7 +582,7 @@
         ).astype(jnp.bfloat16)
         for k in far:
             e = flipped(me, k, ep)
-            push(mine.at[n, e], got.at[n, me], s_out.at[n, k], r_out.at[n, me], e, core)
+            push(mine.at[n, e], got.at[n, me], s_out, r_out.at[n], e, core)
 
     for n in range(pieces):
         at = slice(n * piece, (n + 1) * piece)
@@ -566,27 +591,32 @@
         y = y.reshape(ep, tp, last, piece)
         for i in range(tp):
             sibout[n, i] = y[:, i].astype(jnp.bfloat16)
-        push(sibout.at[n, mate], sibin.at[n], s_sib.at[n], r_sib.at[n], me, mate)
+        push(sibout.at[n, mate], sibin.at[n], s_sib, r_sib.at[n], me, mate)
         if n:
             finish(n - 1)
     finish(pieces - 1)
+    lax.fori_loop(own // 2, own, renew, 0)
     start = pl.multiple_of(lax.rem(me, group) * own, own)
     per = piece // cols
     for n in range(pieces):
+        arrive(got.at[n, pl.ds(0, ep - 1)], r_out.at[n])
         total = mine[n, me].astype(jnp.float32)
-        for k in reversed(far):
-            e = flipped(me, k, ep)
-            arrive(got.at[n, e], r_out.at[n, e])
-            total = total + got[n, e].astype(jnp.float32)
+        for k in far:
+            total = total + got[n, flipped(me, k, ep)].astype(jnp.float32)
         for s in range(per):
             base = res[n * per + s, side, pl.ds(start, own)].astype(jnp.float32)
             base = jnp.where(core == 0, base[:last], base[last:])
             a = n * piece + s * cols
             out[:, a : a + cols] = (base + total[:, s * cols : (s + 1) * cols]).astype(jnp.bfloat16)
-    for send in sends:
-        send.wait_send()
-    for e in range(ep):
-        forward(e).wait_send()
+    arrive(rows_all.at[pl.ds(0, ep - 1)], s_row)
+    arrive(part.at[pl.ds(0, ep - 1)], s_part)
+    arrive(att_all.at[:, pl.ds(0, ep - 1)], s_att)
+    arrive(share.at[pl.ds(0, ep - 1)], s_sh)
+    arrive(psib, s_p)
+    arrive(res.at[pl.ds(0, ep - 1), 0], s_res)
+    arrive(res.at[:, 0], f_res)
+    arrive(sibin, s_sib)
+    arrive(got.at[:, pl.ds(0, ep - 1)], s_out)
 
     @pl.when(jnp.logical_not(here))
     def _():
@@ -594,8 +624,7 @@
 
     @pl.when(here)
     def _():
-        for copy in blocks:
-            copy.wait_send()
+        arrive(xcol.at[pl.ds(0, ep - 1)], s_x)
 
 
 def settle_kernel(tokens, state, out, after, sems):
@@ -616,9 +645,9 @@
     heads = blocks[17].shape[0]
     tiles = cols % 128 == 0 and hidden % 256 == 0 and own % 16 == 0
     tiles = tiles and heads % 8 == 0 and 128 % heads == 0 and heads <= 32
-    tiles = tiles and blocks[0].shape[1] % 2048 == 0 and cols % 256 == 0
+    tiles = tiles and blocks[0].shape[1] % 2048 == 0 and cols == 4 * LANE_WIDTH and own == 16
     ep = lax.axis_size("ep")
-    heads_match = ep & (ep - 1) == 0 and ep > 2 and lax.axis_size("tp") == 2
+    heads_match = ep in (4, 8) and lax.axis_size("tp") == 2
     weights = sum(2 * w.size for w in blocks[18:24])
     rows = own * ep
     held = weights + rows * (12 * blocks[0].shape[1] + 8 * hidden) + 14 * blocks[1].size
@@ -670,9 +699,8 @@
     low, top = forget_narrowing.shape[1], chosen_specialist.shape[1]
     pack = 4
     wide, block_rows = pack * LANE_WIDTH, heads // pack * LANE_WIDTH
-    pieces, batches = 4, 4
+    pieces = 4
     piece, last = width // pieces, own // tp
-    per_head = pltpu.VMEM((own, heads, LANE_WIDTH), f32)
     new_tokens, memory_after = pl.pallas_call(
         functools.partial(layer_kernel, ep, tp, FF_E),
         out_shape=(
@@ -685,25 +713,18 @@
             pltpu.VMEM((own, width), bf16),
             pltpu.VMEM((top, own), jnp.int32),
             pltpu.VMEM((top, own), bf16),
-            pltpu.VMEM((1, width), f32),
-            pltpu.VMEM((1, width), f32),
+            pltpu.VMEM((2, 1, width), f32),
             pltpu.VMEM((width // 128, 128), bf16),
             pltpu.VMEM((width // 128, 128), f32),
             pltpu.VMEM((heads, LANE_WIDTH), f32),
-            pltpu.VMEM((1, half), f32),
-            pltpu.VMEM((low, width), bf16),
-            pltpu.VMEM((low, half), bf16),
-            pltpu.VMEM((1, half), f32),
-            pltpu.VMEM((low, width), bf16),
-            pltpu.VMEM((low, half), bf16),
-            pltpu.VMEM((1, half), f32),
+            pltpu.VMEM((3, 1, half), f32),
+            pltpu.VMEM((2, low, width), bf16),
+            pltpu.VMEM((2, low, half), bf16),
             pltpu.VMEM((3, half, cols), bf16),
             pltpu.VMEM((half, cols), bf16),
-            pltpu.VMEM((width, hidden), bf16),
-            pltpu.VMEM((width, hidden), bf16),
+            pltpu.VMEM((2, width, hidden), bf16),
             pltpu.VMEM((hidden, width), bf16),
-            pltpu.VMEM((dense, width), bf16),
-            pltpu.VMEM((dense, width), bf16),
+            pltpu.VMEM((2, dense, width), bf16),
             pltpu.VMEM((dense, width), bf16),
             pltpu.VMEM((own, block_rows, wide), f32),
             pltpu.VMEM((own, block_rows, wide), bf16),
@@ -711,20 +732,15 @@
             pltpu.VMEM((ep, own, half), bf16),
             pltpu.VMEM((ep, 3, own, cols), bf16),
             pltpu.VMEM((ep, 3, own, cols), bf16),
-            per_head,
-            per_head,
-            per_head,
-            per_head,
-            per_head,
             pltpu.VMEM((own, half), f32),
-            pltpu.VMEM((heads, LANE_WIDTH), f32),
-            pltpu.VMEM((own, 128, LANE_WIDTH), f32),
-            pltpu.VMEM((own, 128, wide), bf16),
-            pltpu.VMEM((own, 128, wide), bf16),
-            pltpu.VMEM((own, block_rows, 128), bf16),
-            per_head,
-            pltpu.VMEM((own, half), bf16),
-            pltpu.VMEM((ep, own, half), bf16),
+            pltpu.VMEM((own, half), f32),
+            pltpu.VMEM((1, half), f32),
+            pltpu.VMEM((wide, wide), bf16),
+            pltpu.VMEM((own, own, wide), bf16),
+            pltpu.VMEM((heads // pack, 128, wide), bf16),
+            pltpu.VMEM((heads // pack, LANE_WIDTH, 128), bf16),
+            pltpu.VMEM((heads // pack, own, wide), bf16),
+            pltpu.VMEM((heads // pack, ep, own, wide), bf16),
             pltpu.VMEM((ep, own, cols), bf16),
             pltpu.VMEM((ep, own, 128), bf16),
             pltpu.VMEM((tp, group * own, cols), bf16),
@@ -742,17 +758,21 @@
             pltpu.VMEM((pieces, ep, last, piece), bf16),
             pltpu.VMEM((pieces, ep, last, piece), bf16),
             pltpu.VMEM((pieces, ep, last, piece), bf16),
-            dma((14,)),
-            dma((batches,)),
-            dma((10,)),
-            *[dma((ep,))] * 10,
+            dma((9,)),
             dma,
+            dma((6,)),
+            *[dma] * 5,
+            dma((group,)),
+            *[dma] * 2,
+            dma((heads // pack,)),
+            *[dma] * 7,
+            dma((ep,)),
             dma,
-            *[dma((ep,))] * 4,
+            dma((ep,)),
+            dma,
             dma((pieces,)),
+            dma,
             dma((pieces,)),
-            dma((pieces, ep)),
-            dma((pieces, ep)),
         ],
         compiler_params=pltpu.CompilerParams(
             collective_id=0, has_side_effects=True, vmem_limit_bytes=54 * 2**20

time: 54.7 us -> 52.5 us (0.960)
  Pallas kernels: 53.9 us -> 51.7 us
    pallas_call x1, Pallas kernels: 50.6 us -> 48.3 us  [kernel_body(): pl.pallas_call(functools.partial(layer_kernel, ep, tp, FF_E), out_shape=(...]
where the time goes in v3:
time: 52.5 us; the launch traced here: 52.3 us
  Pallas kernels  51.7 us (98%)
  between operations  0.65 us (1%)
    pallas_call x1, Pallas kernels, kernel_body(): pl.pallas_call(functools.partial(layer_kernel, ep, tp, FF_E), out_shape=(...  48.3 us
    pallas_call x1, Pallas kernels, kernel_body(): pl.pallas_call(settle_kernel, out_shape=(jax.ShapeDtypeStruct((last, widt...  3.39 us

profile of v3, /device:TPU:0, one launch (start us, length us, event | category | flops | bytes accessed | tf_op | source)
XLA Modules:
  0.0 52.3 jit_solution(8121481406065092791)
XLA Ops:
  0.6 48.3 %layer.1 = (bf16[8,2048]{1,0:T(8,128)(2,1)S(1)}, f32[16,16,64,64]{3,2,1,0:T(8,128)S(1)}) custom-call(bf16[16,2048]{1,0:T(8,128)(2,1)} %x_h.1, f32[16,16,64,64]{3,2,1,0:T(8,128)} %memory.1, s32[2,16]{1,0:T(2,128)} %bitcast.22, bf16[2,16]{1,0:T(2,128)(2,1)} %bitcast.23, f32[1,2048]{1,0:T(1,128)} %bitcast.16, f32[1,2048]{1,0:T(1,128)} %bitcast.17, ...), custom_call_target="tpu_custom_call" | custom-call | tf_op jit(solution)/shard_map/layer/pallas_call | solution.py:704
  48.9 3.4 %settle.1 = (bf16[8,2048]{1,0:T(8,128)(2,1)}, f32[16,16,64,64]{3,2,1,0:T(8,128)}) custom-call(bf16[8,2048]{1,0:T(8,128)(2,1)S(1)} %get-tuple-element.4.tokens, f32[16,16,64,64]{3,2,1,0:T(8,128)S(1)} %get-tuple-element.5.state), custom_call_target="tpu_custom_call" | custom-call | tf_op jit(solution)/shard_map/settle/pallas_call | solution.py:808

commit v4 on v3

--- a/solution.py
+++ b/solution.py
@@ -344,7 +344,6 @@
         )
     share[me] = routes.astype(jnp.bfloat16)
     xcol[me] = x[:, pl.ds(pl.multiple_of(me * cols, cols), cols)]
-    hand_on(rows_all, s_row, r_row, t_row)
     arrive(mem, msem)
     for copy in weights:
         copy.start()
@@ -357,7 +356,9 @@
             pk16[b, at] = joined.astype(jnp.bfloat16)
         return _
 
-    lax.fori_loop(0, own, join, 0)
+    lax.fori_loop(0, own // 2, join, 0)
+    hand_on(rows_all, s_row, r_row, t_row)
+    lax.fori_loop(own // 2, own, join, 0)
 
     arrive(w, wsem.at[0])
     arrive(rows_all.at[pl.ds(0, ep - 2)], r_row)
@@ -435,8 +436,10 @@
         hand_on(att_all.at[j], s_att, r_att, t_att.at[j])
 
     order = [flipped(lax.rem(me, group), j, group) for j in range(packs)]
-    for turn, j in enumerate(order):
-        arrive(gotp.at[pl.ds(0, tp)], r_part.at[j])
+    def channels_of(j):
+        return pl.ds(pl.multiple_of(j * wide, wide), wide)
+
+    def read_out(j):
         sums = []
         for i in range(3):
             total = gotp[j, i].astype(jnp.float32)
@@ -444,10 +447,9 @@
                 total = total + gotp[s * group + j, i].astype(jnp.float32)
             sums.append(total.astype(jnp.bfloat16).astype(jnp.float32))
         q, k, v = sums
-        at = pl.ds(pl.multiple_of(j * wide, wide), wide)
+        at = channels_of(j)
         down = pl.ds(pl.multiple_of(j * LANE_WIDTH, LANE_WIDTH), LANE_WIDTH)
-        r = rch[:, at]
-        scaled = k * r
+        scaled = k * rch[:, at]
         met = scaled * q
         sizes = within(jnp.concatenate([k * k, met, met * wch[:, at]], axis=0))
         inverse = lax.rsqrt(sizes[:own] + 1.0)
@@ -468,14 +470,24 @@
         att[j] = (
             lanes_of(centred * level) * scaling[:, at] + sizes[2 * own :] * v
         ).astype(jnp.bfloat16)
-        spread_out(att.at[j], att_all.at[j], s_att, r_att, t_att.at[j])
+        return acc, v_rows, unit, scaled
+
+    def note(j, acc, v_rows, unit, scaled):
         att_all[j, me] = att[j]
         factors[j] = (
             jnp.concatenate([acc[: pack * own], v_rows], axis=0).T.astype(jnp.bfloat16)
         )
-        moves[j] = stack(-(unit * r), scaled)
-        if turn > 2:
-            pass_att(order[turn - 3])
+        moves[j] = stack(-(unit * rch[:, channels_of(j)]), scaled)
+
+    for some in (order[:2], order[2:]):
+        for j in some:
+            arrive(gotp.at[pl.ds(0, tp)], r_part.at[j])
+        kept = [read_out(j) for j in some]
+        for j in some:
+            spread_out(att.at[j], att_all.at[j], s_att, r_att, t_att.at[j])
+        for j, parts in zip(some, kept):
+            note(j, *parts)
+    pass_att(order[0])
     def renew(b, _):
         for p in range(packs):
             change = jnp.dot(factors[p], only(moves[p], b), preferred_element_type=jnp.float32)

time: 52.5 us -> 52 us (level)
  no operation moved by 1% of the time
where the time goes in v4:
time: 52 us; the launch traced here: 51.9 us
  Pallas kernels  51.2 us (98%)
  between operations  0.65 us (1%)
    pallas_call x1, Pallas kernels, kernel_body(): pl.pallas_call(functools.partial(layer_kernel, ep, tp, FF_E), out_shape=(...  47.8 us
    pallas_call x1, Pallas kernels, kernel_body(): pl.pallas_call(settle_kernel, out_shape=(jax.ShapeDtypeStruct((last, widt...  3.39 us

profile of v4, /device:TPU:0, one launch (start us, length us, event | category | flops | bytes accessed | tf_op | source)
XLA Modules:
  0.0 51.9 jit_solution(13384201444513428574)
XLA Ops:
  0.6 47.8 %layer.1 = (bf16[8,2048]{1,0:T(8,128)(2,1)S(1)}, f32[16,16,64,64]{3,2,1,0:T(8,128)S(1)}) custom-call(bf16[16,2048]{1,0:T(8,128)(2,1)} %x_h.1, f32[16,16,64,64]{3,2,1,0:T(8,128)} %memory.1, s32[2,16]{1,0:T(2,128)} %bitcast.22, bf16[2,16]{1,0:T(2,128)(2,1)} %bitcast.23, f32[1,2048]{1,0:T(1,128)} %bitcast.16, f32[1,2048]{1,0:T(1,128)} %bitcast.17, ...), custom_call_target="tpu_custom_call" | custom-call | tf_op jit(solution)/shard_map/layer/pallas_call | solution.py:716
  48.5 3.4 %settle.1 = (bf16[8,2048]{1,0:T(8,128)(2,1)}, f32[16,16,64,64]{3,2,1,0:T(8,128)}) custom-call(bf16[8,2048]{1,0:T(8,128)(2,1)S(1)} %get-tuple-element.4.tokens, f32[16,16,64,64]{3,2,1,0:T(8,128)S(1)} %get-tuple-element.5.state), custom_call_target="tpu_custom_call" | custom-call | tf_op jit(solution)/shard_map/settle/pallas_call | solution.py:820
